TPU v7x, 32 devices: a whole 2x2x4 slice. The times are simulated.
32 devices in a mesh: sp: 8 (over z, x), tp: 4 (over y, core).
Axes of the slice: x: 2, y: 2, z: 4, core: 2. Of those that a mesh axis runs over, the one named last changes fastest.
Arguments:
- query_rows: bfloat16 [8192, 1024], P('sp', 'tp'), may hold values from -8 to 8
- key_rows: bfloat16 [8192, 1024], P('sp', 'tp'), may hold values from -8 to 8
- value_rows: bfloat16 [8192, 1024], P('sp', 'tp'), may hold values from -6 to 6
- forget_cum: float32 [16, 8192], P('tp', 'sp'), may hold values from -8192 to 0, as said below
- doc_ids: int32 [8192], P('sp'), may hold values from 0 to 3, never falling along the last dimension, each value on 1 to 3072 neighbouring positions
- residual: bfloat16 [8192, 2048], P(('sp', 'tp')), may hold values from -6 to 6
- out_weight: bfloat16 [1024, 2048], replicated, may hold values from -1.5 to 1.5
- norm_gain: float32 [2048], replicated, may hold values from 0.1 to 1.9
- expert_ids: int32 [8192, 2], P(('sp', 'tp')), may hold values from 0 to 7, as said below
- route_weights: float32 [8192, 2], P(('sp', 'tp')), may hold values from 0.2 to 1
- gate_proj: bfloat16 [8, 2048, 512], P('sp'), may hold values from -0.125 to 0.125
- up_proj: bfloat16 [8, 2048, 512], P('sp'), may hold values from -0.125 to 0.125
- down_proj: bfloat16 [8, 512, 2048], P('sp'), may hold values from -0.25 to 0.25
Outputs:
- layer_out: bfloat16 [8192, 2048], P(('sp', 'tp'))
Inputs may be any that keep to these rules, and one draw needn't show every extreme that they name: `forget_cum`: each head's values never rise along the positions. `doc_ids`: document numbers never fall along the positions; a document holds at most 3072 positions, and one holds exactly 3072. `expert_ids`: a token's 2 experts differ and lie in one group of 4 consecutive experts; among the 256 rows of one device no expert is named more than 160 times, and in every draw one expert is named exactly 160 times by the rows of every device.
All inputs are finite; a program needn't handle non-finite values.
Results may differ from a plain program's by a relative error of at most 0.0054.
Values may be sent and summed in bfloat16 or wider, within the bound.
No kernel may reach another device: no remote copies, remote signals or barrier semaphores. Data moves between devices by JAX's collectives and lax.ppermute only.
A program may use at most 128 MiB of HBM per device.

v0:
```python
import functools

import jax
import jax.numpy as jnp
from jax import lax
from jax.experimental import pallas as pl
from jax.experimental.pallas import tpu as pltpu
from jax.sharding import PartitionSpec as P


REACH = 3
LANES = 128
norm_eps = 1e-06
LOW = -1e30
VMEM_LIMIT = 32 * 1024 * 1024


def attend_kernel(
    low_ref, full_ref, pick_ref, q_ref, *refs, sources, own, heads_pair, block_k, scale,
):
    i = pl.program_id(0)
    block_q = q_ref.shape[0]
    count = sum(sources)
    k_refs, v_refs = refs[:count], refs[count : 2 * count]
    gate_ref, kdoc_ref, qdoc_ref = refs[2 * count : 2 * count + 3]
    state = refs[2 * count + 3 : -4]
    k_all, v_all, m_ref, acc_ref = refs[-4:]
    tok = k_refs[0].shape[0]
    head_size = LANES // heads_pair

    @pl.when(i == 0)
    def _():
        v_all[:, LANES:] = jnp.ones((v_all.shape[0], LANES), v_all.dtype)

        def fill(place, k_src, v_src):
            rows = pl.ds(place * tok, tok)
            k_all[rows, :] = k_src[...]
            v_all[rows, :LANES] = v_src[...]

        at = 0
        for place, options in enumerate(sources):
            if options == 1:
                fill(place, k_refs[at], v_refs[at])
            else:
                for o in range(options):
                    pl.when(pick_ref[0] == o)(
                        functools.partial(fill, place, k_refs[at + o], v_refs[at + o])
                    )
            at += options

    low, full = low_ref[i], full_ref[i]
    lane = lax.broadcasted_iota(jnp.int32, (block_q, LANES), 1)
    query = q_ref[...].astype(jnp.float32) * scale
    mine = [(lane // head_size) == h for h in range(heads_pair)]
    q_heads = [jnp.where(x, query, 0.0).astype(jnp.bfloat16) for x in mine]
    for h in range(heads_pair):
        if own:
            m_ref[h] = jnp.full((block_q, LANES), LOW, jnp.float32)
            acc_ref[h] = jnp.zeros((block_q, 2 * LANES), jnp.float32)
        else:
            m_ref[h] = jnp.broadcast_to(
                state[2][:, h * head_size : h * head_size + 1], (block_q, LANES)
            )
            acc_ref[h, :, :LANES] = state[0][...]
            acc_ref[h, :, LANES:] = state[1][...]

    def step(j, masked, causal):
        start = pl.multiple_of(j * block_k, block_k)
        rows = pl.ds(start, block_k)
        if masked:
            allowed = qdoc_ref[...] == kdoc_ref[:, rows]
            if causal:
                shape = (block_q, block_k)
                q_pos = i * block_q + lax.broadcasted_iota(jnp.int32, shape, 0)
                k_pos = start + lax.broadcasted_iota(jnp.int32, shape, 1)
                allowed = allowed & (k_pos <= q_pos)
        for h in range(heads_pair):
            score = lax.dot_general(
                q_heads[h], k_all[rows, :], (((1,), (1,)), ((), ())),
                preferred_element_type=jnp.float32,
            )
            score = score - gate_ref[0, h : h + 1, rows]
            if masked:
                score = jnp.where(allowed, score, LOW)
            before = m_ref[h]
            top = jnp.maximum(before, jnp.max(score, axis=1, keepdims=True))
            shrink = jnp.exp(before - top)
            m_ref[h] = top
            wide = jnp.concatenate([top] * (block_k // LANES), axis=1)
            expo = jnp.exp(score - wide).astype(jnp.bfloat16)
            product = jnp.dot(expo, v_all[rows, :], preferred_element_type=jnp.float32)
            acc_ref[h] = acc_ref[h] * jnp.concatenate([shrink, shrink], axis=1) + product

    def loop(first, end, masked, causal):
        def body(j, carry):
            step(j, masked, causal)
            return carry

        lax.fori_loop(first, end, body, 0)

    if own:
        loop(low, (i * block_q + block_q + block_k - 1) // block_k, True, True)
    else:
        loop(low, full, True, False)
        loop(full, len(sources) * tok // block_k, False, False)
    summed, total, top = (
        functools.reduce(
            lambda x, h: jnp.where(mine[h], parts[h], x), range(1, heads_pair), parts[0]
        )
        for parts in (
            [acc_ref[h, :, :LANES] for h in range(heads_pair)],
            [acc_ref[h, :, LANES:] for h in range(heads_pair)],
            [m_ref[h] for h in range(heads_pair)],
        )
    )
    if own:
        state[0][...] = summed
        state[1][...] = total
        state[2][...] = top
    else:
        state[3][...] = (summed / total).astype(state[3].dtype)


BLOCK_Q = 512
BLOCK_K = 512


def visible(key_docs, docs):
    block_q, block_k = min(BLOCK_Q, docs.shape[0]), min(BLOCK_K, docs.shape[0])
    blocked = key_docs.reshape(-1, block_k)
    query_docs = docs.reshape(-1, block_q)
    low = jnp.sum(blocked[None, :, -1] < query_docs[:, None, 0], axis=1).astype(jnp.int32)
    full = jnp.sum(blocked[None, :, 0] < query_docs[:, None, -1], axis=1).astype(jnp.int32)
    return low, full


def attend(pair, query_rows, blocks, sources, pick, bounds, gates, key_docs, docs, head_size, state):
    own = state is None
    tok = query_rows.shape[0]
    span = gates.shape[2]
    block_q, block_k = min(BLOCK_Q, tok), min(BLOCK_K, tok)
    nq = tok // block_q
    heads_pair = LANES // head_size
    slab = pl.BlockSpec((block_q, LANES), lambda i, *_: (i, 0))
    saved = jax.ShapeDtypeStruct((tok, LANES), jnp.float32)

    def column(at):
        return pl.BlockSpec((tok, LANES), lambda i, *_: (at, pair))

    return pl.pallas_call(
        functools.partial(
            attend_kernel,
            sources=sources,
            own=own,
            heads_pair=heads_pair,
            block_k=block_k,
            scale=head_size ** (-0.5),
        ),
        out_shape=[saved] * 3 if own else jax.ShapeDtypeStruct((tok, LANES), jnp.bfloat16),
        grid_spec=pltpu.PrefetchScalarGridSpec(
            num_scalar_prefetch=3,
            grid=(nq,),
            in_specs=[pl.BlockSpec((block_q, LANES), lambda i, *_: (i, pair))]
            + [column(x[1]) for x in blocks]
            + [column(x[3]) for x in blocks]
            + [
                pl.BlockSpec((1, heads_pair, span), lambda i, *_: (i, 0, 0)),
                pl.BlockSpec((1, span), lambda i, *_: (0, 0)),
                pl.BlockSpec((block_q, 1), lambda i, *_: (i, 0)),
            ]
            + ([] if own else [slab] * 3),
            out_specs=[slab] * 3 if own else slab,
            scratch_shapes=[
                pltpu.VMEM((span, LANES), jnp.bfloat16),
                pltpu.VMEM((span, 2 * LANES), jnp.bfloat16),
                pltpu.VMEM((heads_pair, block_q, LANES), jnp.float32),
                pltpu.VMEM((heads_pair, block_q, 2 * LANES), jnp.float32),
            ],
        ),
        compiler_params=pltpu.CompilerParams(vmem_limit_bytes=VMEM_LIMIT),
        cost_estimate=pl.CostEstimate(
            flops=16 * tok * span * LANES, bytes_accessed=12 * tok * LANES, transcendentals=0
        ),
        name="attend_own" if own else "attend_rest",
    )(
        *bounds, pick, query_rows, *[x[0] for x in blocks], *[x[2] for x in blocks],
        gates[:, pair * heads_pair : (pair + 1) * heads_pair], key_docs[None, :], docs[:, None],
        *(() if own else state),
    )


def send(x, axis, pairs):
    return lax.ppermute(x, axis, pairs)


def mix_kernel(info_ref, *refs, offsets, pairs):
    count = len(offsets)
    slabs, pieces = refs[: count * pairs], refs[count * pairs : count * (pairs + 1)]
    weight_ref, gain_ref, normed_ref, own_ref, hidden = refs[count * (pairs + 1) :]
    model = weight_ref.shape[1]
    width = weight_ref.shape[0] // count
    chunk = min(512, model)
    t = info_ref[0]
    j = pl.program_id(0)
    for i, offset in enumerate(offsets):

        @pl.when((t ^ j) == offset)
        def _(piece=pieces[i]):
            hidden[...] = piece[:, :model].astype(jnp.float32)

    heads = [
        jnp.concatenate([x[...] for x in slabs[i * pairs : (i + 1) * pairs]], axis=1)
        for i in range(count)
    ]
    squares = jnp.zeros((hidden.shape[0], LANES), jnp.float32)
    for c in range(0, model, chunk):
        total = hidden[:, c : c + chunk]
        for i in range(count):
            rows = pl.ds(pl.multiple_of((t ^ offsets[i]) * width, width), width)
            total = total + jnp.dot(
                heads[i], weight_ref[rows, c : c + chunk], preferred_element_type=jnp.float32
            )
        hidden[:, c : c + chunk] = total
        for l in range(0, chunk, LANES):
            squares = squares + total[:, l : l + LANES] * total[:, l : l + LANES]
    mean = jnp.sum(squares, axis=1, keepdims=True) * (1.0 / model)
    factor = lax.rsqrt(mean + norm_eps)
    for c in range(0, model, chunk):
        normed_ref[:, c : c + chunk] = (
            hidden[:, c : c + chunk] * factor * gain_ref[:, c : c + chunk]
        ).astype(normed_ref.dtype)

    @pl.when(t == j)
    def _():
        own_ref[...] = hidden[...]


def mix(t, offsets, pieces, rows, out_weight, norm_gain):
    tok_loc, wide_model = rows[0].shape
    model = out_weight.shape[1]
    parts = len(offsets)
    pairs = len(pieces[0])
    vmem = lambda shape: pl.BlockSpec(shape, lambda j, *_: (0, 0))
    return pl.pallas_call(
        functools.partial(mix_kernel, offsets=offsets, pairs=pairs),
        out_shape=[
            jax.ShapeDtypeStruct((parts * tok_loc, model), jnp.bfloat16),
            jax.ShapeDtypeStruct((tok_loc, model), jnp.float32),
        ],
        grid_spec=pltpu.PrefetchScalarGridSpec(
            num_scalar_prefetch=1,
            grid=(parts,),
            in_specs=[pl.BlockSpec((tok_loc, LANES), lambda j, *_: (j, 0))] * (parts * pairs)
            + [vmem((tok_loc, wide_model))] * parts
            + [vmem(out_weight.shape), vmem((1, model))],
            out_specs=[pl.BlockSpec((tok_loc, model), lambda j, *_: (j, 0)), vmem((tok_loc, model))],
            scratch_shapes=[pltpu.VMEM((tok_loc, model), jnp.float32)],
        ),
        compiler_params=pltpu.CompilerParams(vmem_limit_bytes=VMEM_LIMIT * 3 // 2),
        cost_estimate=pl.CostEstimate(
            flops=2 * parts * tok_loc * out_weight.size, bytes_accessed=16 << 20, transcendentals=0
        ),
        name="mix",
    )(
        t[None], *[y for x in pieces for y in x], *rows, out_weight, norm_gain[None],
    )


def act_block(x, parts_of, weight):
    depth = x.shape[1] // len(parts_of)
    product = jnp.dot(x[:, :depth], parts_of[0][...], preferred_element_type=jnp.float32)
    for i, part in enumerate(parts_of[1:], 1):
        product = product + jnp.dot(
            x[:, i * depth : (i + 1) * depth], part[...], preferred_element_type=jnp.float32
        )
    piece = product.shape[1] // 2
    gate, up = product[:, :piece], product[:, piece:]
    act = gate / (1.0 + jnp.exp(-gate)) * up
    return (act * weight).astype(jnp.bfloat16)


def acts_kernel(x_ref, weight_ref, *refs, first):
    out_ref = refs[-1]
    x = x_ref[...]
    out_ref[...] = jnp.concatenate(
        [
            act_block(x, [ref], weight_ref[:, first + i : first + i + 1])
            for i, ref in enumerate(refs[:-1])
        ],
        axis=1,
    )


def acts_of(normed, weights, first, shards):
    tok, model = normed.shape
    rows = min(256, tok)
    piece = shards[0].shape[1] // 2
    return pl.pallas_call(
        functools.partial(acts_kernel, first=first),
        out_shape=jax.ShapeDtypeStruct((tok, piece * len(shards)), jnp.bfloat16),
        grid=(tok // rows,),
        in_specs=[
            pl.BlockSpec((rows, model), lambda i: (i, 0)),
            pl.BlockSpec((rows, weights.shape[1]), lambda i: (i, 0)),
        ]
        + [pl.BlockSpec(x.shape, lambda i: (0, 0)) for x in shards],
        out_specs=pl.BlockSpec((rows, piece * len(shards)), lambda i: (i, 0)),
        compiler_params=pltpu.CompilerParams(vmem_limit_bytes=VMEM_LIMIT),
        cost_estimate=pl.CostEstimate(
            flops=4 * tok * model * piece * len(shards),
            bytes_accessed=2 * (normed.size + len(shards) * shards[0].size),
            transcendentals=0,
        ),
        name="acts",
    )(normed, weights, *shards)


def early_kernel(*refs, groups):
    acts, downs = refs[:groups], refs[groups:-2]
    out_ref, down_all = refs[-2:]
    piece = downs[0].shape[0]

    @pl.when(pl.program_id(0) == 0)
    def _():
        for i, x in enumerate(downs):
            down_all[pl.ds(i * piece, piece), :] = x[...]

    rows = jnp.concatenate([x[...] for x in acts], axis=1)
    chunk = min(512, out_ref.shape[1])
    for c in range(0, out_ref.shape[1], chunk):
        out_ref[:, c : c + chunk] = jnp.dot(
            rows, down_all[:, c : c + chunk], preferred_element_type=jnp.float32
        )


def early_sums(acts, downs):
    tok, (piece, model) = acts[0].shape[0], downs[0].shape
    rows = min(256, tok)
    return pl.pallas_call(
        functools.partial(early_kernel, groups=len(acts)),
        out_shape=jax.ShapeDtypeStruct((tok, model), jnp.float32),
        grid=(tok // rows,),
        in_specs=[pl.BlockSpec((rows, x.shape[1]), lambda i: (i, 0)) for x in acts]
        + [pl.BlockSpec(x.shape, lambda i: (0, 0)) for x in downs],
        out_specs=pl.BlockSpec((rows, model), lambda i: (i, 0)),
        scratch_shapes=[pltpu.VMEM((piece * len(downs), model), jnp.bfloat16)],
        compiler_params=pltpu.CompilerParams(vmem_limit_bytes=VMEM_LIMIT),
        cost_estimate=pl.CostEstimate(
            flops=2 * tok * piece * len(downs) * model, bytes_accessed=16 << 20, transcendentals=0
        ),
        name="early",
    )(*acts, *downs)


def last_kernel(block_ref, x_ref, weight_ref, early_ref, *refs, at, halves):
    wide, flat, out_ref = refs[:halves], refs[halves:-1], refs[-1]
    act = act_block(x_ref[...], wide, weight_ref[:, at : at + 1])
    lower = jnp.concatenate([x[...] for x in flat], axis=0)
    total = early_ref[...] + jnp.dot(act, lower, preferred_element_type=jnp.float32)
    out_ref[...] = total.astype(out_ref.dtype)


def last_sums(blocks, rows, normed, weights, at, early, wide, flat, dtype):
    model = normed.shape[1]
    pick = lambda g, block_ref: (block_ref[g], 0)
    whole = lambda x: pl.BlockSpec(x.shape, lambda g, *_: (0, 0))
    return pl.pallas_call(
        functools.partial(last_kernel, at=at, halves=len(wide)),
        out_shape=jax.ShapeDtypeStruct((blocks.shape[0] * rows, model), dtype),
        grid_spec=pltpu.PrefetchScalarGridSpec(
            num_scalar_prefetch=1,
            grid=(blocks.shape[0],),
            in_specs=[
                pl.BlockSpec((rows, model), pick),
                pl.BlockSpec((rows, weights.shape[1]), pick),
                pl.BlockSpec((rows, model), pick),
            ]
            + [whole(x) for x in (*wide, *flat)],
            out_specs=pl.BlockSpec((rows, model), lambda g, *_: (g, 0)),
        ),
        compiler_params=pltpu.CompilerParams(vmem_limit_bytes=VMEM_LIMIT),
        cost_estimate=pl.CostEstimate(
            flops=2 * blocks.shape[0] * rows * model * 384, bytes_accessed=8 << 20, transcendentals=0
        ),
        name="last",
    )(blocks, normed, weights, early, *wide, *flat)


def three_parts(x):
    high = lax.reduce_precision(x, 8, 7)
    middle = lax.reduce_precision(x - high, 8, 7)
    low = x - high - middle
    return [y.astype(jnp.bfloat16) for y in (high, middle, low)]


def per_device(
    query_rows, key_rows, value_rows, forget_cum, doc_ids, residual, out_weight, norm_gain,
    expert_ids, route_weights, gate_proj, up_proj, down_proj,
):
    n = lax.axis_size("sp")
    parts = lax.axis_size("tp")
    s = lax.axis_index("sp")
    t = lax.axis_index("tp")
    tok, width = query_rows.shape
    heads = forget_cum.shape[0]
    head_size = width // heads
    tok_loc, model = residual.shape
    hidden_units = gate_proj.shape[2]
    piece = hidden_units // parts

    after = lax.optimization_barrier
    flip = lambda bit: [(i, i ^ bit) for i in range(parts)]

    def behind(x):
        one = send(x, "sp", [(i, i + 1) for i in range(n - 1)])
        two = send(x, "sp", [(i, i + 2) for i in range(n - 2)])
        far = send(one, "sp", [(i, i + 2) for i in range(0, n - 2, 2)])
        side = send(two, "sp", [(i, i + 1) for i in range(0, n - 1, 2)])
        return side, far, two, one

    key_blocks = behind(key_rows)
    marks = jnp.concatenate([*three_parts(forget_cum), doc_ids[None].astype(jnp.bfloat16)])
    marks = jnp.pad(marks, ((0, 4 * heads - marks.shape[0]), (0, 0))).reshape(-1, width)
    value_blocks = behind(jnp.concatenate([value_rows, marks], axis=0))
    odd = s % 2 == 1

    def expert_at(place):
        place = (place + n) % n
        return jnp.where(place < (n + 1) // 2, 2 * place, 2 * (n - 1 - place) + 1)

    order = list(range(0, n, 2)) + list(range(1, n, 2))[::-1]
    forward = [(order[i], order[(i + 1) % n]) for i in range(n)]
    backward = [(b, a) for a, b in forward]
    place = jnp.where(s % 2 == 0, s // 2, n - 1 - s // 2)
    gate_up = jnp.concatenate(
        [
            lax.dynamic_slice_in_dim(gate_proj[0], t * piece, piece, 1),
            lax.dynamic_slice_in_dim(up_proj[0], t * piece, piece, 1),
        ],
        axis=1,
    )
    down = lax.dynamic_slice_in_dim(down_proj[0], t * piece, piece, 0)

    def ring(k, ahead, back):
        if 2 * k < n:
            return send(ahead, "sp", forward), send(back, "sp", backward)
        half = ahead.shape[0] // 2
        return send(ahead[:half], "sp", forward), send(back[half:], "sp", backward)

    steps = n // 2
    wide = {1: ring(1, gate_up, gate_up)}
    flat = {1: ring(1, down, down)}

    routes = jnp.concatenate([expert_ids.astype(jnp.bfloat16), *three_parts(route_weights)], axis=1)
    routes = jnp.pad(routes, ((0, 0), (0, LANES - routes.shape[1])))
    bits = [1 << b for b in range(parts.bit_length() - 1)]
    group = [(0, jnp.concatenate([residual, routes], axis=1))]
    for bit in bits[::-1]:
        group = group + [(o ^ bit, send(x, "tp", flip(bit))) for o, x in group]
    tail = jnp.zeros((tok, LANES), jnp.bfloat16)
    for o, x in group:
        tail = lax.dynamic_update_slice_in_dim(tail, x[:, model:], (t ^ o) * tok_loc, 0)
    topk = expert_ids.shape[1]
    tail = tail.astype(jnp.float32)
    group_ids = tail[:, :topk]
    group_weights = (
        tail[:, topk : 2 * topk] + tail[:, 2 * topk : 3 * topk] + tail[:, 3 * topk : 4 * topk]
    )
    places = [place] + [place + d for k in range(1, (n + 1) // 2) for d in (-k, k)]
    places += [place + n // 2] * (n % 2 == 0)
    arriving = jnp.stack([expert_at(x) for x in places]).astype(jnp.float32)
    weights = jnp.sum(
        jnp.where(group_ids[:, :, None] == arriving[None, None, :], group_weights[:, :, None], 0.0),
        axis=1,
    )

    nq = tok // min(BLOCK_Q, tok)
    pairs = width // LANES
    origin = forget_cum.reshape(heads, nq, tok // nq)[:, :, 0].T[:, :, None]
    docs = doc_ids.astype(jnp.float32)
    pick = jnp.where(odd, 0, 1).astype(jnp.int32)[None]
    own_bounds = visible(docs, docs)
    states = []
    for p in range(pairs):
        states.append(
            attend(
                p, query_rows, [(key_rows, 0, value_rows, 0)], (1,), pick, own_bounds,
                forget_cum[None] - origin, docs, docs, head_size, None,
            )
        )
    side, far, two, one = [x[tok:] for x in value_blocks]
    sent = [x.reshape(-1, tok).astype(jnp.float32) for x in (jnp.where(odd, side, far), two, one)]
    earlier = jnp.concatenate(
        [x[:heads] + x[heads : 2 * heads] + x[2 * heads : 3 * heads] for x in sent], axis=1
    )
    earlier_docs = jnp.concatenate(
        [jnp.where(REACH - i <= s, x[3 * heads], -1.0) for i, x in enumerate(sent)]
    )
    bounds = visible(earlier_docs, docs)
    relative = earlier[None] - origin
    attended = []
    for p in range(pairs):
        attended.append(
            attend(
                p, query_rows, [(x, 0, y, 0) for x, y in zip(key_blocks, value_blocks)],
                (2, 1, 1), pick, bounds, relative, earlier_docs, docs, head_size, states[p],
            )
        )
    wide[2] = ring(2, *wide[1])
    flat[2] = ring(2, *flat[1])

    pieces = [(0, tuple(attended))]
    for bit in bits[::-1]:
        pieces = pieces + [(o ^ bit, tuple(send(y, "tp", flip(bit)) for y in x)) for o, x in pieces]
    offsets = tuple(o for o, _ in pieces)
    normed, own_hidden = mix(
        t, offsets, [x for _, x in pieces], [x for _, x in group], out_weight, norm_gain
    )

    for k in range(3, steps + 1):
        wide[k] = ring(k, *wide[k - 1])
        flat[k] = ring(k, *flat[k - 1])
    acts, downs, first = [], [down], 0
    for k in range(1, steps):
        shards = [gate_up] * (k == 1) + list(wide[k])
        acts.append(acts_of(normed, weights, first, shards))
        first += len(shards)
        downs += list(flat[k])
    early = early_sums(acts, downs)

    def sums(offsets, dtype):
        blocks = jnp.stack([t ^ o for o in offsets]).astype(jnp.int32)
        return last_sums(
            blocks, tok_loc, normed, weights, first, early, wide[steps], flat[steps], dtype
        )

    keep = [0]
    for bit in bits[::-1][:-1]:
        keep = keep + [o ^ bit for o in keep]
    away = sums([o ^ bits[0] for o in keep], jnp.bfloat16)
    moved = send(away, "tp", flip(bits[0])).astype(jnp.float32)
    kept = sums(keep, jnp.float32)
    totals = {
        o: kept[i * tok_loc : (i + 1) * tok_loc] + moved[i * tok_loc : (i + 1) * tok_loc]
        for i, o in enumerate(keep)
    }
    totals[0] = totals[0] + own_hidden
    for bit in bits[1:]:
        for offset in [o for o in totals if o & bit]:
            moved = send(totals.pop(offset).astype(jnp.bfloat16), "tp", flip(bit))
            ready, moved = after((totals[offset ^ bit], moved))
            totals[offset ^ bit] = ready + moved.astype(jnp.float32)
    return totals[0].astype(jnp.bfloat16)


def solution(mesh):
    placed = (
        P("sp", "tp"),
        P("sp", "tp"),
        P("sp", "tp"),
        P("tp", "sp"),
        P("sp"),
        P(("sp", "tp"), None),
        P(),
        P(),
        P(("sp", "tp"), None),
        P(("sp", "tp"), None),
        P("sp", None, None),
        P("sp", None, None),
        P("sp", None, None),
    )
    return jax.shard_map(
        per_device, mesh=mesh, in_specs=placed, out_specs=P(("sp", "tp"), None), check_vma=False
    )
```

profile of v0, /device:TPU:0, one launch (start us, length us, event | category | flops | bytes accessed | tf_op | source)
XLA Modules:
  0.0 258.5 jit_solution(5592433114666824835)
XLA Ops:
  4.2 5.8 %collective-permute-start = (bf16[1088,256]{1,0:T(8,128)(2,1)}, bf16[1088,256]{1,0:T(8,128)(2,1)}, u32[]{:S(2)}, u32[]{:S(2)}) collective-permute-start(bf16[1088,256]{1,0:T(8,128)(2,1)} %constant_dynamic-update-slice_fusion), channel_id=1, source_target_pairs={{0,8},{4,12},{8,16},{12,20},{16,24},{20,28},{1,9},{5,13},{9,17},{1... | collective-permute-start | bytes 1671176 | tf_op jit(solution)/shard_map/ppermute | solution.py:193
  10.0 4.2 %collective-permute-start.2 = (bf16[1088,256]{1,0:T(8,128)(2,1)}, bf16[1088,256]{1,0:T(8,128)(2,1)}, u32[]{:S(2)}, u32[]{:S(2)}) collective-permute-start(bf16[1088,256]{1,0:T(8,128)(2,1)} %constant_dynamic-update-slice_fusion), channel_id=1, source_target_pairs={{0,4},{4,8},{8,12},{12,16},{16,20},{20,24},{24,28},{1,5},{5,9},{9,... | collective-permute-start | bytes 1671176 | tf_op jit(solution)/shard_map/ppermute | solution.py:193
  16.9 4.2 %collective-permute-start.6 = (bf16[1024,256]{1,0:T(8,128)(2,1)}, bf16[1024,256]{1,0:T(8,128)(2,1)}, u32[]{:S(2)}, u32[]{:S(2)}) collective-permute-start(bf16[1024,256]{1,0:T(8,128)(2,1)} %refs_0_.3), channel_id=1, source_target_pairs={{0,4},{4,8},{8,12},{12,16},{16,20},{20,24},{24,28},{1,5},{5,9},{9,... | collective-permute-start | bytes 1572872 | tf_op jit(solution)/shard_map/ppermute | solution.py:193
  26.3 5.2 %attend_own.3 = (f32[1024,128]{1,0:T(8,128)S(1)}, f32[1024,128]{1,0:T(8,128)S(1)}, f32[1024,128]{1,0:T(8,128)S(1)}) custom-call(s32[2]{0:T(128)S(1)} %get-tuple-element.30.low_ref, s32[2]{0:T(128)S(1)} %get-tuple-element.29.full_ref, s32[1]{0:T(128)} %bitcast.2.pick_ref, bf16[1024,256]{1,0:T(8,128)(2,1)S(1)} %copy-done.8, bf16[1024,256]{1,0:T(8,128)(2,1)S(1)} %copy-done.7, ...), custom_call_target="tpu_custom_call" | custom-call | flops 2147483648 | bytes 1572864 | tf_op jit(solution)/shard_map/attend_own/pallas_call | solution.py:150
  33.9 5.2 %attend_own.2 = (f32[1024,128]{1,0:T(8,128)S(1)}, f32[1024,128]{1,0:T(8,128)S(1)}, f32[1024,128]{1,0:T(8,128)S(1)}) custom-call(s32[2]{0:T(128)S(1)} %get-tuple-element.30.low_ref, s32[2]{0:T(128)S(1)} %get-tuple-element.29.full_ref, s32[1]{0:T(128)} %bitcast.2.pick_ref, bf16[1024,256]{1,0:T(8,128)(2,1)S(1)} %copy-done.8, bf16[1024,256]{1,0:T(8,128)(2,1)S(1)} %copy-done.7, ...), custom_call_target="tpu_custom_call" | custom-call | flops 2147483648 | bytes 1572864 | tf_op jit(solution)/shard_map/attend_own/pallas_call | solution.py:150
  43.2 4.7 %collective-permute-start.1 = (bf16[1088,256]{1,0:T(8,128)(2,1)}, bf16[1088,256]{1,0:T(8,128)(2,1)}, u32[]{:S(2)}, u32[]{:S(2)}) collective-permute-start(bf16[1088,256]{1,0:T(8,128)(2,1)} %collective-permute-done.refs_6_), channel_id=1, source_target_pairs={{0,4},{8,12},{16,20},{24,28},{1,5},{9,13},{17,21},{25,29},{2,6},{1... | collective-permute-start | bytes 1671176 | tf_op jit(solution)/shard_map/ppermute | solution.py:193
  50.7 7.2 %collective-permute-done.1.refs_4_ = bf16[1088,256]{1,0:T(8,128)(2,1)} collective-permute-done((bf16[1088,256]{1,0:T(8,128)(2,1)}, bf16[1088,256]{1,0:T(8,128)(2,1)}, u32[]{:S(2)}, u32[]{:S(2)}) %collective-permute-start.1) | collective-permute-done | bytes 557088 | tf_op jit(solution)/shard_map/ppermute | solution.py:193
  69.6 3.4 %collective-permute-done.24.refs_5_ = bf16[128,2048]{1,0:T(8,128)(2,1)} collective-permute-done((bf16[128,2048]{1,0:T(8,128)(2,1)}, bf16[128,2048]{1,0:T(8,128)(2,1)}, u32[]{:S(2)}, u32[]{:S(2)}) %collective-permute-start.24) | collective-permute-done | bytes 524320 | tf_op jit(solution)/shard_map/ppermute | solution.py:193
  73.0 7.8 %collective-permute-done.5.refs_0_ = bf16[1024,256]{1,0:T(8,128)(2,1)S(1)} collective-permute-done((bf16[1024,256]{1,0:T(8,128)(2,1)}, bf16[1024,256]{1,0:T(8,128)(2,1)S(1)}, u32[]{:S(2)}, u32[]{:S(2)}) %collective-permute-start.5) | collective-permute-done | bytes 524320 | tf_op jit(solution)/shard_map/ppermute | solution.py:193
  84.4 12.7 %collective-permute-done.7.refs_1_ = bf16[1024,256]{1,0:T(8,128)(2,1)} collective-permute-done((bf16[1024,256]{1,0:T(8,128)(2,1)}, bf16[1024,256]{1,0:T(8,128)(2,1)}, u32[]{:S(2)}, u32[]{:S(2)}) %collective-permute-start.7) | collective-permute-done | bytes 524320 | tf_op jit(solution)/shard_map/ppermute | solution.py:193
  104.9 3.1 %attend_rest.3.refs_1_ = bf16[1024,128]{1,0:T(8,128)(2,1)S(1)} custom-call(s32[2]{0:T(128)S(1)} %get-tuple-element.47.low_ref, s32[2]{0:T(128)S(1)} %get-tuple-element.48.full_ref, s32[1]{0:T(128)} %bitcast.2.pick_ref, bf16[1024,256]{1,0:T(8,128)(2,1)S(1)} %copy-done.9, bf16[1024,256]{1,0:T(8,128)(2,1)S(1)} %copy-done.15, ...), custom_call_target="tpu_custom_call" | custom-call | flops 6442450944 | bytes 1572864 | tf_op jit(solution)/shard_map/attend_rest/pallas_call | solution.py:150
  108.0 10.5 %collective-permute-start.19 = (bf16[2048,256]{1,0:T(8,128)(2,1)}, bf16[2048,256]{1,0:T(8,128)(2,1)}, u32[]{:S(2)}, u32[]{:S(2)}) collective-permute-start(bf16[2048,256]{1,0:T(8,128)(2,1)} %collective-permute-done.17.refs_1_), channel_id=1, source_target_pairs={{0,8},{8,16},{16,24},{24,28},{28,20},{20,12},{12,4},{4,0},{1,9},{9... | collective-permute-start | bytes 3145736 | tf_op jit(solution)/shard_map/ppermute | solution.py:193
  120.1 5.8 %collective-permute-start.27 = (bf16[128,2048]{1,0:T(8,128)(2,1)S(1)}, bf16[128,2048]{1,0:T(8,128)(2,1)S(1)}, u32[]{:S(2)}, u32[]{:S(2)}) collective-permute-start(bf16[128,2048]{1,0:T(8,128)(2,1)S(1)} %collective-permute-done.25.refs_6_), channel_id=1, source_target_pairs={{0,8},{8,16},{16,24},{24,28},{28,20},{20,12},{12,4},{4,0},{1,9},{9... | collective-permute-start | bytes 1572872 | tf_op jit(solution)/shard_map/ppermute | solution.py:193
  125.9 3.7 %attend_rest.2.refs_0_ = bf16[1024,128]{1,0:T(8,128)(2,1)} custom-call(s32[2]{0:T(128)S(1)} %get-tuple-element.47.low_ref, s32[2]{0:T(128)S(1)} %get-tuple-element.48.full_ref, s32[1]{0:T(128)} %bitcast.2.pick_ref, bf16[1024,256]{1,0:T(8,128)(2,1)S(1)} %copy-done.9, bf16[1024,256]{1,0:T(8,128)(2,1)S(1)} %copy-done.16, ...), custom_call_target="tpu_custom_call" | custom-call | flops 6442450944 | bytes 1572864 | tf_op jit(solution)/shard_map/attend_rest/pallas_call | solution.py:150
  129.6 23.4 %collective-permute-done.27.refs_8_ = bf16[128,2048]{1,0:T(8,128)(2,1)S(1)} collective-permute-done((bf16[128,2048]{1,0:T(8,128)(2,1)S(1)}, bf16[128,2048]{1,0:T(8,128)(2,1)S(1)}, u32[]{:S(2)}, u32[]{:S(2)}) %collective-permute-start.27) | collective-permute-done | bytes 524320 | tf_op jit(solution)/shard_map/ppermute | solution.py:193
  169.6 8.9 %collective-permute-start.31 = (bf16[64,2048]{1,0:T(8,128)(2,1)}, bf16[64,2048]{1,0:T(8,128)(2,1)S(1)}, u32[]{:S(2)}, u32[]{:S(2)}) collective-permute-start(bf16[64,2048]{1,0:T(8,128)(2,1)} %slice.208), channel_id=1, source_target_pairs={{0,8},{8,16},{16,24},{24,28},{28,20},{20,12},{12,4},{4,0},{1,9},{9... | collective-permute-start | bytes 786440 | tf_op jit(solution)/shard_map/ppermute | solution.py:193
  179.4 11.9 %mix.1 = (bf16[1024,2048]{1,0:T(8,128)(2,1)}, f32[256,2048]{1,0:T(8,128)}) custom-call(s32[1]{0:T(128)} %bitcast.info_ref, bf16[1024,128]{1,0:T(8,128)(2,1)} %attend_rest.2.refs_0_, bf16[1024,128]{1,0:T(8,128)(2,1)S(1)} %attend_rest.3.refs_1_, bf16[1024,128]{1,0:T(8,128)(2,1)} %collective-permute-done.8.refs_2_, ...), custom_call_target="tpu_custom_call" | custom-call | flops 4294967296 | bytes 16777216 | tf_op jit(solution)/shard_map/mix/pallas_call | solution.py:244
  193.5 4.5 %acts.4.refs_1_ = bf16[1024,256]{1,0:T(8,128)(2,1)S(1)} custom-call(bf16[1024,2048]{1,0:T(8,128)(2,1)S(1)} %copy-done.2, f32[1024,8]{1,0:T(8,128)S(1)} %copy.66.weight_ref, bf16[2048,256]{1,0:T(8,128)(2,1)} %collective-permute-done.19.refs_0_, bf16[2048,256]{1,0:T(8,128)(2,1)} %collective-permute-done.20.refs_1_), custom_call_target="tpu_custom_call" | custom-call | flops 2147483648 | bytes 6291456 | tf_op jit(solution)/shard_map/acts/pallas_call | solution.py:298
  198.0 5.7 %acts.3.refs_0_ = bf16[1024,384]{1,0:T(8,128)(2,1)S(1)} custom-call(bf16[1024,2048]{1,0:T(8,128)(2,1)S(1)} %copy-done.2, f32[1024,8]{1,0:T(8,128)S(1)} %copy.66.weight_ref, bf16[2048,256]{1,0:T(8,128)(2,1)S(1)} %pad_maximum_fusion.1.refs_0_, bf16[2048,256]{1,0:T(8,128)(2,1)} %collective-permute-done.17.refs_1_, bf16[2048,256]{1,0:T(8,128)(2,1)} %collective-permute-done.18.refs_2_), custom_call_target="tpu_custom_call" | custom-call | flops 3221225472 | bytes 7340032 | tf_op jit(solution)/shard_map/acts/pallas_call | solution.py:298
  208.6 4.7 %acts.5.refs_2_ = bf16[1024,256]{1,0:T(8,128)(2,1)S(1)} custom-call(bf16[1024,2048]{1,0:T(8,128)(2,1)S(1)} %copy-done.2, f32[1024,8]{1,0:T(8,128)S(1)} %copy.66.weight_ref, bf16[2048,256]{1,0:T(8,128)(2,1)} %collective-permute-done.21.refs_0_, bf16[2048,256]{1,0:T(8,128)(2,1)} %collective-permute-done.22.refs_1_), custom_call_target="tpu_custom_call" | custom-call | flops 2147483648 | bytes 6291456 | tf_op jit(solution)/shard_map/acts/pallas_call | solution.py:298
  213.3 7.1 %early.1.early_ref = f32[1024,2048]{1,0:T(8,128)S(1)} custom-call(bf16[1024,384]{1,0:T(8,128)(2,1)S(1)} %acts.3.refs_0_, bf16[1024,256]{1,0:T(8,128)(2,1)S(1)} %acts.4.refs_1_, bf16[1024,256]{1,0:T(8,128)(2,1)S(1)} %acts.5.refs_2_, bf16[128,2048]{1,0:T(8,128)(2,1)} %dynamic-slice_bitcast_fusion.refs_3_, bf16[128,2048]{1,0:T(8,128)(2,1)} %collective-permute-done.23.refs_4_, ...), custom_call_target="tpu_custom_call" | custom-call | flops 3758096384 | bytes 16777216 | tf_op jit(solution)/shard_map/early/pallas_call | solution.py:339
  221.6 3.2 %last.3 = bf16[512,2048]{1,0:T(8,128)(2,1)S(1)} custom-call(s32[2]{0:T(128)S(1)} %pad_add_fusion.1.block_ref, bf16[1024,2048]{1,0:T(8,128)(2,1)S(1)} %copy-done.3, f32[1024,8]{1,0:T(8,128)S(1)} %copy.66.weight_ref, f32[1024,2048]{1,0:T(8,128)S(1)} %early.1.early_ref, bf16[1024,256]{1,0:T(8,128)(2,1)S(1)} %collective-permute-done.29.refs_0_, ...), custom_call_target="tpu_custom_call" | custom-call | flops 805306368 | bytes 8388608 | tf_op jit(solution)/shard_map/last/pallas_call | solution.py:367
  225.0 3.2 %last.2 = f32[512,2048]{1,0:T(8,128)S(1)} custom-call(s32[2]{0:T(128)S(1)} %pad_add_fusion.block_ref, bf16[1024,2048]{1,0:T(8,128)(2,1)S(1)} %copy-done.3, f32[1024,8]{1,0:T(8,128)S(1)} %copy.66.weight_ref, f32[1024,2048]{1,0:T(8,128)S(1)} %early.1.early_ref, bf16[1024,256]{1,0:T(8,128)(2,1)S(1)} %collective-permute-done.29.refs_0_, ...), custom_call_target="tpu_custom_call" | custom-call | flops 805306368 | bytes 8388608 | tf_op jit(solution)/shard_map/last/pallas_call | solution.py:367
  232.1 24.5 %collective-permute-done.34 = bf16[256,2048]{1,0:T(8,128)(2,1)S(1)} collective-permute-done((bf16[256,2048]{1,0:T(8,128)(2,1)S(1)}, bf16[256,2048]{1,0:T(8,128)(2,1)S(1)}, u32[]{:S(2)}, u32[]{:S(2)}) %collective-permute-start.34) | collective-permute-done | bytes 1048608 | tf_op jit(solution)/shard_map/ppermute | solution.py:193
  (208 shorter events, 77.3 us)
Async XLA Ops:
  4.2 37.4 %collective-permute-start = (bf16[1088,256]{1,0:T(8,128)(2,1)}, bf16[1088,256]{1,0:T(8,128)(2,1)}, u32[]{:S(2)}, u32[]{:S(2)}) collective-permute-start(bf16[1088,256]{1,0:T(8,128)(2,1)} %constant_dynamic-update-slice_fusion), channel_id=1, source_target_pairs={{0,8},{4,12},{8,16},{12,20},{16,24},{20,28},{1,9},{5,13},{9,17},{1... | collective-permute-start | bytes 1671176 | tf_op jit(solution)/shard_map/ppermute | solution.py:193
  10.0 32.4 %collective-permute-start.2 = (bf16[1088,256]{1,0:T(8,128)(2,1)}, bf16[1088,256]{1,0:T(8,128)(2,1)}, u32[]{:S(2)}, u32[]{:S(2)}) collective-permute-start(bf16[1088,256]{1,0:T(8,128)(2,1)} %constant_dynamic-update-slice_fusion), channel_id=1, source_target_pairs={{0,4},{4,8},{8,12},{12,16},{16,20},{20,24},{24,28},{1,5},{5,9},{9,... | collective-permute-start | bytes 1671176 | tf_op jit(solution)/shard_map/ppermute | solution.py:193
  14.2 48.6 %collective-permute-start.4 = (bf16[1024,256]{1,0:T(8,128)(2,1)}, bf16[1024,256]{1,0:T(8,128)(2,1)}, u32[]{:S(2)}, u32[]{:S(2)}) collective-permute-start(bf16[1024,256]{1,0:T(8,128)(2,1)} %refs_0_.3), channel_id=1, source_target_pairs={{0,8},{4,12},{8,16},{12,20},{16,24},{20,28},{1,9},{5,13},{9,17},{1... | collective-permute-start | bytes 1572872 | tf_op jit(solution)/shard_map/ppermute | solution.py:193
  16.9 48.3 %collective-permute-start.6 = (bf16[1024,256]{1,0:T(8,128)(2,1)}, bf16[1024,256]{1,0:T(8,128)(2,1)}, u32[]{:S(2)}, u32[]{:S(2)}) collective-permute-start(bf16[1024,256]{1,0:T(8,128)(2,1)} %refs_0_.3), channel_id=1, source_target_pairs={{0,4},{4,8},{8,12},{12,16},{16,20},{20,24},{24,28},{1,5},{5,9},{9,... | collective-permute-start | bytes 1572872 | tf_op jit(solution)/shard_map/ppermute | solution.py:193
  22.0 44.9 %collective-permute-start.23 = (bf16[128,2048]{1,0:T(8,128)(2,1)}, bf16[128,2048]{1,0:T(8,128)(2,1)}, u32[]{:S(2)}, u32[]{:S(2)}) collective-permute-start(bf16[128,2048]{1,0:T(8,128)(2,1)} %dynamic-slice_bitcast_fusion.refs_3_), channel_id=1, source_target_pairs={{0,8},{8,16},{16,24},{24,28},{28,20},{20,12},{12,4},{4,0},{1,9},{9... | collective-permute-start | bytes 1572872 | tf_op jit(solution)/shard_map/ppermute | solution.py:193
  60.4 39.2 %collective-permute-start.14 = (bf16[256,2176]{1,0:T(8,128)(2,1)S(1)}, bf16[256,2176]{1,0:T(8,128)(2,1)}, u32[]{:S(2)}, u32[]{:S(2)}) collective-permute-start(bf16[256,2176]{1,0:T(8,128)(2,1)S(1)} %pad_maximum_fusion.refs_8_), channel_id=1, source_target_pairs={{0,2},{1,3},{2,0},{3,1},{4,6},{5,7},{6,4},{7,5},{8,10},{9,11},{10,... | collective-permute-start | bytes 3342344 | tf_op jit(solution)/shard_map/ppermute | solution.py:193
  62.8 36.8 %collective-permute-start.17 = (bf16[2048,256]{1,0:T(8,128)(2,1)S(1)}, bf16[2048,256]{1,0:T(8,128)(2,1)}, u32[]{:S(2)}, u32[]{:S(2)}) collective-permute-start(bf16[2048,256]{1,0:T(8,128)(2,1)S(1)} %pad_maximum_fusion.1.refs_0_), channel_id=1, source_target_pairs={{0,8},{8,16},{16,24},{24,28},{28,20},{20,12},{12,4},{4,0},{1,9},{9... | collective-permute-start | bytes 3145736 | tf_op jit(solution)/shard_map/ppermute | solution.py:193
  65.2 15.6 %collective-permute-start.5 = (bf16[1024,256]{1,0:T(8,128)(2,1)}, bf16[1024,256]{1,0:T(8,128)(2,1)S(1)}, u32[]{:S(2)}, u32[]{:S(2)}) collective-permute-start(bf16[1024,256]{1,0:T(8,128)(2,1)} %collective-permute-done.4.refs_2_), channel_id=1, source_target_pairs={{0,4},{8,12},{16,20},{24,28},{1,5},{9,13},{17,21},{25,29},{2,6},{1... | collective-permute-start | bytes 1572872 | tf_op jit(solution)/shard_map/ppermute | solution.py:193
  66.9 30.2 %collective-permute-start.7 = (bf16[1024,256]{1,0:T(8,128)(2,1)}, bf16[1024,256]{1,0:T(8,128)(2,1)}, u32[]{:S(2)}, u32[]{:S(2)}) collective-permute-start(bf16[1024,256]{1,0:T(8,128)(2,1)} %collective-permute-done.6.refs_3_), channel_id=1, source_target_pairs={{0,8},{8,16},{16,24},{1,9},{9,17},{17,25},{2,10},{10,18},{18,26},{... | collective-permute-start | bytes 1572872 | tf_op jit(solution)/shard_map/ppermute | solution.py:193
  73.0 52.8 %collective-permute-start.15 = (bf16[256,2176]{1,0:T(8,128)(2,1)S(1)}, bf16[256,2176]{1,0:T(8,128)(2,1)}, u32[]{:S(2)}, u32[]{:S(2)}) collective-permute-start(bf16[256,2176]{1,0:T(8,128)(2,1)S(1)} %pad_maximum_fusion.refs_8_), channel_id=1, source_target_pairs={{0,1},{1,0},{2,3},{3,2},{4,5},{5,4},{6,7},{7,6},{8,9},{9,8},{10,11... | collective-permute-start | bytes 3342344 | tf_op jit(solution)/shard_map/ppermute | solution.py:193
  81.6 26.4 %collective-permute-start.18 = (bf16[2048,256]{1,0:T(8,128)(2,1)S(1)}, bf16[2048,256]{1,0:T(8,128)(2,1)}, u32[]{:S(2)}, u32[]{:S(2)}) collective-permute-start(bf16[2048,256]{1,0:T(8,128)(2,1)S(1)} %pad_maximum_fusion.1.refs_0_), channel_id=1, source_target_pairs={{8,0},{16,8},{24,16},{28,24},{20,28},{12,20},{4,12},{0,4},{9,1},{1... | collective-permute-start | bytes 3145736 | tf_op jit(solution)/shard_map/ppermute | solution.py:193
  97.1 21.4 %collective-permute-start.25 = (bf16[128,2048]{1,0:T(8,128)(2,1)}, bf16[128,2048]{1,0:T(8,128)(2,1)S(1)}, u32[]{:S(2)}, u32[]{:S(2)}) collective-permute-start(bf16[128,2048]{1,0:T(8,128)(2,1)} %collective-permute-done.23.refs_4_), channel_id=1, source_target_pairs={{0,8},{8,16},{16,24},{24,28},{28,20},{20,12},{12,4},{4,0},{1,9},{9... | collective-permute-start | bytes 1572872 | tf_op jit(solution)/shard_map/ppermute | solution.py:193
  99.6 20.5 %collective-permute-start.26 = (bf16[128,2048]{1,0:T(8,128)(2,1)}, bf16[128,2048]{1,0:T(8,128)(2,1)S(1)}, u32[]{:S(2)}, u32[]{:S(2)}) collective-permute-start(bf16[128,2048]{1,0:T(8,128)(2,1)} %collective-permute-done.24.refs_5_), channel_id=1, source_target_pairs={{8,0},{16,8},{24,16},{28,24},{20,28},{12,20},{4,12},{0,4},{9,1},{1... | collective-permute-start | bytes 1572872 | tf_op jit(solution)/shard_map/ppermute | solution.py:193
  99.6 55.8 %collective-permute-start.16 = (bf16[256,2176]{1,0:T(8,128)(2,1)}, bf16[256,2176]{1,0:T(8,128)(2,1)S(1)}, u32[]{:S(2)}, u32[]{:S(2)}) collective-permute-start(bf16[256,2176]{1,0:T(8,128)(2,1)} %collective-permute-done.14.refs_9_), channel_id=1, source_target_pairs={{0,1},{1,0},{2,3},{3,2},{4,5},{5,4},{6,7},{7,6},{8,9},{9,8},{10,11... | collective-permute-start | bytes 3342344 | tf_op jit(solution)/shard_map/ppermute | solution.py:193
  108.0 59.0 %collective-permute-start.19 = (bf16[2048,256]{1,0:T(8,128)(2,1)}, bf16[2048,256]{1,0:T(8,128)(2,1)}, u32[]{:S(2)}, u32[]{:S(2)}) collective-permute-start(bf16[2048,256]{1,0:T(8,128)(2,1)} %collective-permute-done.17.refs_1_), channel_id=1, source_target_pairs={{0,8},{8,16},{16,24},{24,28},{28,20},{20,12},{12,4},{4,0},{1,9},{9... | collective-permute-start | bytes 3145736 | tf_op jit(solution)/shard_map/ppermute | solution.py:193
  118.5 50.7 %collective-permute-start.20 = (bf16[2048,256]{1,0:T(8,128)(2,1)}, bf16[2048,256]{1,0:T(8,128)(2,1)}, u32[]{:S(2)}, u32[]{:S(2)}) collective-permute-start(bf16[2048,256]{1,0:T(8,128)(2,1)} %collective-permute-done.18.refs_2_), channel_id=1, source_target_pairs={{8,0},{16,8},{24,16},{28,24},{20,28},{12,20},{4,12},{0,4},{9,1},{1... | collective-permute-start | bytes 3145736 | tf_op jit(solution)/shard_map/ppermute | solution.py:193
  120.1 33.0 %collective-permute-start.27 = (bf16[128,2048]{1,0:T(8,128)(2,1)S(1)}, bf16[128,2048]{1,0:T(8,128)(2,1)S(1)}, u32[]{:S(2)}, u32[]{:S(2)}) collective-permute-start(bf16[128,2048]{1,0:T(8,128)(2,1)S(1)} %collective-permute-done.25.refs_6_), channel_id=1, source_target_pairs={{0,8},{8,16},{16,24},{24,28},{28,20},{20,12},{12,4},{4,0},{1,9},{9... | collective-permute-start | bytes 1572872 | tf_op jit(solution)/shard_map/ppermute | solution.py:193
  125.8 29.5 %collective-permute-start.28 = (bf16[128,2048]{1,0:T(8,128)(2,1)S(1)}, bf16[128,2048]{1,0:T(8,128)(2,1)}, u32[]{:S(2)}, u32[]{:S(2)}) collective-permute-start(bf16[128,2048]{1,0:T(8,128)(2,1)S(1)} %collective-permute-done.26.refs_7_), channel_id=1, source_target_pairs={{8,0},{16,8},{24,16},{28,24},{20,28},{12,20},{4,12},{0,4},{9,1},{1... | collective-permute-start | bytes 1572872 | tf_op jit(solution)/shard_map/ppermute | solution.py:193
  167.0 36.7 %collective-permute-start.21 = (bf16[2048,256]{1,0:T(8,128)(2,1)}, bf16[2048,256]{1,0:T(8,128)(2,1)}, u32[]{:S(2)}, u32[]{:S(2)}) collective-permute-start(bf16[2048,256]{1,0:T(8,128)(2,1)} %collective-permute-done.19.refs_0_), channel_id=1, source_target_pairs={{0,8},{8,16},{16,24},{24,28},{28,20},{20,12},{12,4},{4,0},{1,9},{9... | collective-permute-start | bytes 3145736 | tf_op jit(solution)/shard_map/ppermute | solution.py:193
  169.2 38.0 %collective-permute-start.22 = (bf16[2048,256]{1,0:T(8,128)(2,1)}, bf16[2048,256]{1,0:T(8,128)(2,1)}, u32[]{:S(2)}, u32[]{:S(2)}) collective-permute-start(bf16[2048,256]{1,0:T(8,128)(2,1)} %collective-permute-done.20.refs_1_), channel_id=1, source_target_pairs={{8,0},{16,8},{24,16},{28,24},{20,28},{12,20},{4,12},{0,4},{9,1},{1... | collective-permute-start | bytes 3145736 | tf_op jit(solution)/shard_map/ppermute | solution.py:193
  169.6 50.9 %collective-permute-start.31 = (bf16[64,2048]{1,0:T(8,128)(2,1)}, bf16[64,2048]{1,0:T(8,128)(2,1)S(1)}, u32[]{:S(2)}, u32[]{:S(2)}) collective-permute-start(bf16[64,2048]{1,0:T(8,128)(2,1)} %slice.208), channel_id=1, source_target_pairs={{0,8},{8,16},{16,24},{24,28},{28,20},{20,12},{12,4},{4,0},{1,9},{9... | collective-permute-start | bytes 786440 | tf_op jit(solution)/shard_map/ppermute | solution.py:193
  178.4 42.0 %collective-permute-start.32 = (bf16[64,2048]{1,0:T(8,128)(2,1)}, bf16[64,2048]{1,0:T(8,128)(2,1)S(1)}, u32[]{:S(2)}, u32[]{:S(2)}) collective-permute-start(bf16[64,2048]{1,0:T(8,128)(2,1)} %slice.209), channel_id=1, source_target_pairs={{8,0},{16,8},{24,16},{28,24},{20,28},{12,20},{4,12},{0,4},{9,1},{1... | collective-permute-start | bytes 786440 | tf_op jit(solution)/shard_map/ppermute | solution.py:193
  204.8 15.7 %collective-permute-start.29 = (bf16[1024,256]{1,0:T(8,128)(2,1)S(1)}, bf16[1024,256]{1,0:T(8,128)(2,1)S(1)}, u32[]{:S(2)}, u32[]{:S(2)}) collective-permute-start(bf16[1024,256]{1,0:T(8,128)(2,1)S(1)} %slice.206), channel_id=1, source_target_pairs={{0,8},{8,16},{16,24},{24,28},{28,20},{20,12},{12,4},{4,0},{1,9},{9... | collective-permute-start | bytes 1572872 | tf_op jit(solution)/shard_map/ppermute | solution.py:193
  230.9 25.6 %collective-permute-start.34 = (bf16[256,2048]{1,0:T(8,128)(2,1)S(1)}, bf16[256,2048]{1,0:T(8,128)(2,1)S(1)}, u32[]{:S(2)}, u32[]{:S(2)}) collective-permute-start(bf16[256,2048]{1,0:T(8,128)(2,1)S(1)} %get-tuple-element.31), channel_id=1, source_target_pairs={{0,2},{1,3},{2,0},{3,1},{4,6},{5,7},{6,4},{7,5},{8,10},{9,11},{10,... | collective-permute-start | bytes 3145736 | tf_op jit(solution)/shard_map/ppermute | solution.py:193
  (49 other events, 438.2 us)
where the time goes:
time: 260 us; the launch traced here: 259 us
  waiting for transfers between devices  83 us (32%)
  starting transfers between devices  73.3 us (28%)
  Pallas kernels  57.4 us (22%)
  local copies, waits for them, and re-layouts  35.8 us (14%)
  other arithmetic  8.28 us (3%)
    ppermute x35, waiting for transfers between devices, send(): return lax.ppermute(x, axis, pairs)  83 us
    ppermute x35, starting transfers between devices, send(): return lax.ppermute(x, axis, pairs)  73.3 us
    unnamed x81, local copies, waits for them, and re-layouts  18 us
    pallas_call x4, Pallas kernels, attend(): pl.pallas_call(functools.partial(attend_kernel, sources=sources, own=own,...  17.2 us
    pallas_call x3, Pallas kernels, acts_of(): pl.pallas_call(functools.partial(acts_kernel, first=first), out_shape=jax...  14.8 us
    pallas_call x1, Pallas kernels, mix(): pl.pallas_call(functools.partial(mix_kernel, offsets=offsets, pairs=pairs...  11.9 us
    pallas_call x1, Pallas kernels, early_sums(): pl.pallas_call(functools.partial(early_kernel, groups=len(acts)), out_sha...  7.09 us
    pallas_call x2, Pallas kernels, last_sums(): pl.pallas_call(functools.partial(last_kernel, at=at, halves=len(wide)), o...  6.36 us
  transfers between devices with their start and end apart: 35, of which 10 were waited for; matrix products, arithmetic and copies ran while one was open for 8% of the time, Pallas kernels for 21%

commit v1 on v0

--- a/solution.py
+++ b/solution.py
@@ -537,13 +537,15 @@
     keep = [0]
     for bit in bits[::-1][:-1]:
         keep = keep + [o ^ bit for o in keep]
-    away = sums([o ^ bits[0] for o in keep], jnp.bfloat16)
-    moved = send(away, "tp", flip(bits[0])).astype(jnp.float32)
-    kept = sums(keep, jnp.float32)
-    totals = {
-        o: kept[i * tok_loc : (i + 1) * tok_loc] + moved[i * tok_loc : (i + 1) * tok_loc]
-        for i, o in enumerate(keep)
-    }
+    totals = {}
+    for chosen in (bits[1], 0):
+        group = [o for o in keep if o & bits[1] == chosen]
+        away = sums([o ^ bits[0] for o in group], jnp.bfloat16)
+        moved = send(away, "tp", flip(bits[0])).astype(jnp.float32)
+        kept = sums(group, jnp.float32)
+        for i, o in enumerate(group):
+            rows = slice(i * tok_loc, (i + 1) * tok_loc)
+            totals[o] = kept[rows] + moved[rows]
     totals[0] = totals[0] + own_hidden
     for bit in bits[1:]:
         for offset in [o for o in totals if o & bit]:

time: 260 us -> 257 us (0.988)
  waiting for transfers between devices: 83 us -> 79.9 us
    ppermute x35 -> x36, waiting for transfers between devices: 83 us -> 79.9 us  [send(): return lax.ppermute(x, axis, pairs)]
    ppermute x35 -> x36, starting transfers between devices: 73.3 us -> 75.8 us  [send(): return lax.ppermute(x, axis, pairs)]
    pallas_call x2 -> x4, Pallas kernels: 6.36 us -> 5.21 us  [last_sums(): pl.pallas_call(functools.partial(last_kernel, at=at, halves=len(wide)), o...]
    unnamed x81 -> x77, local copies, waits for them, and re-layouts: 18 us -> 17.3 us
  transfers between devices with their start and end apart: 35 -> 36, of which waited for: 10 -> 11; matrix products, arithmetic and copies ran while one was open for 8% -> 9% of each run, Pallas kernels for 21% -> 21%
where the time goes in v1:
time: 257 us; the launch traced here: 255 us
  waiting for transfers between devices  79.9 us (31%)
  starting transfers between devices  75.8 us (29%)
  Pallas kernels  56.1 us (22%)
  local copies, waits for them, and re-layouts  35.2 us (14%)
  other arithmetic  7.17 us (3%)
    ppermute x36, waiting for transfers between devices, send(): return lax.ppermute(x, axis, pairs)  79.9 us
    ppermute x36, starting transfers between devices, send(): return lax.ppermute(x, axis, pairs)  75.8 us
    unnamed x77, local copies, waits for them, and re-layouts  17.3 us
    pallas_call x4, Pallas kernels, attend(): pl.pallas_call(functools.partial(attend_kernel, sources=sources, own=own,...  17.2 us
    pallas_call x3, Pallas kernels, acts_of(): pl.pallas_call(functools.partial(acts_kernel, first=first), out_shape=jax...  14.7 us
    pallas_call x1, Pallas kernels, mix(): pl.pallas_call(functools.partial(mix_kernel, offsets=offsets, pairs=pairs...  11.9 us
    pallas_call x1, Pallas kernels, early_sums(): pl.pallas_call(functools.partial(early_kernel, groups=len(acts)), out_sha...  7.07 us
    dynamic_update_slice x5, local copies, waits for them, and re-layouts, per_device(): lax.dynamic_update_slice_in_dim(tail, x[:, model:], (t ^ o) * tok_loc, 0)  5.56 us
  transfers between devices with their start and end apart: 36, of which 11 were waited for; matrix products, arithmetic and copies ran while one was open for 9% of the time, Pallas kernels for 21%

profile of v1, /device:TPU:0, one launch (start us, length us, event | category | flops | bytes accessed | tf_op | source)
XLA Modules:
  0.0 255.2 jit_solution(17753275481462109203)
XLA Ops:
  4.2 5.7 %collective-permute-start.2 = (bf16[1088,256]{1,0:T(8,128)(2,1)}, bf16[1088,256]{1,0:T(8,128)(2,1)}, u32[]{:S(2)}, u32[]{:S(2)}) collective-permute-start(bf16[1088,256]{1,0:T(8,128)(2,1)} %constant_dynamic-update-slice_fusion), channel_id=1, source_target_pairs={{0,4},{4,8},{8,12},{12,16},{16,20},{20,24},{24,28},{1,5},{5,9},{9,... | collective-permute-start | bytes 1671176 | tf_op jit(solution)/shard_map/ppermute | solution.py:193
  9.9 3.5 %collective-permute-start = (bf16[1088,256]{1,0:T(8,128)(2,1)}, bf16[1088,256]{1,0:T(8,128)(2,1)}, u32[]{:S(2)}, u32[]{:S(2)}) collective-permute-start(bf16[1088,256]{1,0:T(8,128)(2,1)} %constant_dynamic-update-slice_fusion), channel_id=1, source_target_pairs={{0,8},{4,12},{8,16},{12,20},{16,24},{20,28},{1,9},{5,13},{9,17},{1... | collective-permute-start | bytes 1671176 | tf_op jit(solution)/shard_map/ppermute | solution.py:193
  13.4 3.5 %collective-permute-start.4 = (bf16[1024,256]{1,0:T(8,128)(2,1)}, bf16[1024,256]{1,0:T(8,128)(2,1)}, u32[]{:S(2)}, u32[]{:S(2)}) collective-permute-start(bf16[1024,256]{1,0:T(8,128)(2,1)} %refs_0_.3), channel_id=1, source_target_pairs={{0,8},{4,12},{8,16},{12,20},{16,24},{20,28},{1,9},{5,13},{9,17},{1... | collective-permute-start | bytes 1572872 | tf_op jit(solution)/shard_map/ppermute | solution.py:193
  16.9 4.3 %collective-permute-start.6 = (bf16[1024,256]{1,0:T(8,128)(2,1)}, bf16[1024,256]{1,0:T(8,128)(2,1)}, u32[]{:S(2)}, u32[]{:S(2)}) collective-permute-start(bf16[1024,256]{1,0:T(8,128)(2,1)} %refs_0_.3), channel_id=1, source_target_pairs={{0,4},{4,8},{8,12},{12,16},{16,20},{20,24},{24,28},{1,5},{5,9},{9,... | collective-permute-start | bytes 1572872 | tf_op jit(solution)/shard_map/ppermute | solution.py:193
  25.7 5.2 %attend_own.2 = (f32[1024,128]{1,0:T(8,128)S(1)}, f32[1024,128]{1,0:T(8,128)S(1)}, f32[1024,128]{1,0:T(8,128)S(1)}) custom-call(s32[2]{0:T(128)S(1)} %get-tuple-element.30.low_ref, s32[2]{0:T(128)S(1)} %get-tuple-element.29.full_ref, s32[1]{0:T(128)} %bitcast.1.pick_ref, bf16[1024,256]{1,0:T(8,128)(2,1)S(1)} %copy-done.6, bf16[1024,256]{1,0:T(8,128)(2,1)S(1)} %copy-done.5, ...), custom_call_target="tpu_custom_call" | custom-call | flops 2147483648 | bytes 1572864 | tf_op jit(solution)/shard_map/attend_own/pallas_call | solution.py:150
  33.3 5.2 %attend_own.3 = (f32[1024,128]{1,0:T(8,128)S(1)}, f32[1024,128]{1,0:T(8,128)S(1)}, f32[1024,128]{1,0:T(8,128)S(1)}) custom-call(s32[2]{0:T(128)S(1)} %get-tuple-element.30.low_ref, s32[2]{0:T(128)S(1)} %get-tuple-element.29.full_ref, s32[1]{0:T(128)} %bitcast.1.pick_ref, bf16[1024,256]{1,0:T(8,128)(2,1)S(1)} %copy-done.6, bf16[1024,256]{1,0:T(8,128)(2,1)S(1)} %copy-done.5, ...), custom_call_target="tpu_custom_call" | custom-call | flops 2147483648 | bytes 1572864 | tf_op jit(solution)/shard_map/attend_own/pallas_call | solution.py:150
  44.7 4.1 %collective-permute-start.1 = (bf16[1088,256]{1,0:T(8,128)(2,1)}, bf16[1088,256]{1,0:T(8,128)(2,1)}, u32[]{:S(2)}, u32[]{:S(2)}) collective-permute-start(bf16[1088,256]{1,0:T(8,128)(2,1)} %collective-permute-done.refs_6_), channel_id=1, source_target_pairs={{0,4},{8,12},{16,20},{24,28},{1,5},{9,13},{17,21},{25,29},{2,6},{1... | collective-permute-start | bytes 1671176 | tf_op jit(solution)/shard_map/ppermute | solution.py:193
  48.9 10.0 %collective-permute-done.3.refs_5_ = bf16[1088,256]{1,0:T(8,128)(2,1)} collective-permute-done((bf16[1088,256]{1,0:T(8,128)(2,1)}, bf16[1088,256]{1,0:T(8,128)(2,1)}, u32[]{:S(2)}, u32[]{:S(2)}) %collective-permute-start.3) | collective-permute-done | bytes 557088 | tf_op jit(solution)/shard_map/ppermute | solution.py:193
  66.4 4.7 %collective-permute-start.7 = (bf16[1024,256]{1,0:T(8,128)(2,1)}, bf16[1024,256]{1,0:T(8,128)(2,1)}, u32[]{:S(2)}, u32[]{:S(2)}) collective-permute-start(bf16[1024,256]{1,0:T(8,128)(2,1)} %collective-permute-done.6.refs_3_), channel_id=1, source_target_pairs={{0,8},{8,16},{16,24},{1,9},{9,17},{17,25},{2,10},{10,18},{18,26},{... | collective-permute-start | bytes 1572872 | tf_op jit(solution)/shard_map/ppermute | solution.py:193
  72.3 8.9 %collective-permute-done.5.refs_0_ = bf16[1024,256]{1,0:T(8,128)(2,1)S(1)} collective-permute-done((bf16[1024,256]{1,0:T(8,128)(2,1)}, bf16[1024,256]{1,0:T(8,128)(2,1)S(1)}, u32[]{:S(2)}, u32[]{:S(2)}) %collective-permute-start.5) | collective-permute-done | bytes 524320 | tf_op jit(solution)/shard_map/ppermute | solution.py:193
  84.8 11.4 %collective-permute-done.7.refs_1_ = bf16[1024,256]{1,0:T(8,128)(2,1)} collective-permute-done((bf16[1024,256]{1,0:T(8,128)(2,1)}, bf16[1024,256]{1,0:T(8,128)(2,1)}, u32[]{:S(2)}, u32[]{:S(2)}) %collective-permute-start.7) | collective-permute-done | bytes 524320 | tf_op jit(solution)/shard_map/ppermute | solution.py:193
  104.1 3.7 %attend_rest.2.refs_0_ = bf16[1024,128]{1,0:T(8,128)(2,1)} custom-call(s32[2]{0:T(128)S(1)} %get-tuple-element.45.low_ref, s32[2]{0:T(128)S(1)} %get-tuple-element.46.full_ref, s32[1]{0:T(128)} %bitcast.1.pick_ref, bf16[1024,256]{1,0:T(8,128)(2,1)S(1)} %copy-done.7, bf16[1024,256]{1,0:T(8,128)(2,1)S(1)} %copy-done.13, ...), custom_call_target="tpu_custom_call" | custom-call | flops 6442450944 | bytes 1572864 | tf_op jit(solution)/shard_map/attend_rest/pallas_call | solution.py:150
  108.2 10.1 %collective-permute-start.19 = (bf16[2048,256]{1,0:T(8,128)(2,1)}, bf16[2048,256]{1,0:T(8,128)(2,1)}, u32[]{:S(2)}, u32[]{:S(2)}) collective-permute-start(bf16[2048,256]{1,0:T(8,128)(2,1)} %collective-permute-done.17.refs_1_), channel_id=1, source_target_pairs={{0,8},{8,16},{16,24},{24,28},{28,20},{20,12},{12,4},{4,0},{1,9},{9... | collective-permute-start | bytes 3145736 | tf_op jit(solution)/shard_map/ppermute | solution.py:193
  119.8 7.8 %collective-permute-start.27 = (bf16[128,2048]{1,0:T(8,128)(2,1)S(1)}, bf16[128,2048]{1,0:T(8,128)(2,1)}, u32[]{:S(2)}, u32[]{:S(2)}) collective-permute-start(bf16[128,2048]{1,0:T(8,128)(2,1)S(1)} %collective-permute-done.25.refs_6_), channel_id=1, source_target_pairs={{0,8},{8,16},{16,24},{24,28},{28,20},{20,12},{12,4},{4,0},{1,9},{9... | collective-permute-start | bytes 1572872 | tf_op jit(solution)/shard_map/ppermute | solution.py:193
  127.7 3.1 %attend_rest.3.refs_1_ = bf16[1024,128]{1,0:T(8,128)(2,1)S(1)} custom-call(s32[2]{0:T(128)S(1)} %get-tuple-element.45.low_ref, s32[2]{0:T(128)S(1)} %get-tuple-element.46.full_ref, s32[1]{0:T(128)} %bitcast.1.pick_ref, bf16[1024,256]{1,0:T(8,128)(2,1)S(1)} %copy-done.7, bf16[1024,256]{1,0:T(8,128)(2,1)S(1)} %copy-done.14, ...), custom_call_target="tpu_custom_call" | custom-call | flops 6442450944 | bytes 1572864 | tf_op jit(solution)/shard_map/attend_rest/pallas_call | solution.py:150
  130.8 22.0 %collective-permute-done.27.refs_8_ = bf16[128,2048]{1,0:T(8,128)(2,1)} collective-permute-done((bf16[128,2048]{1,0:T(8,128)(2,1)S(1)}, bf16[128,2048]{1,0:T(8,128)(2,1)}, u32[]{:S(2)}, u32[]{:S(2)}) %collective-permute-start.27) | collective-permute-done | bytes 524320 | tf_op jit(solution)/shard_map/ppermute | solution.py:193
  167.8 2.6 %collective-permute-start.21 = (bf16[2048,256]{1,0:T(8,128)(2,1)}, bf16[2048,256]{1,0:T(8,128)(2,1)}, u32[]{:S(2)}, u32[]{:S(2)}) collective-permute-start(bf16[2048,256]{1,0:T(8,128)(2,1)} %collective-permute-done.19.refs_0_), channel_id=1, source_target_pairs={{0,8},{8,16},{16,24},{24,28},{28,20},{20,12},{12,4},{4,0},{1,9},{9... | collective-permute-start | bytes 3145736 | tf_op jit(solution)/shard_map/ppermute | solution.py:193
  170.7 9.9 %collective-permute-start.31 = (bf16[64,2048]{1,0:T(8,128)(2,1)}, bf16[64,2048]{1,0:T(8,128)(2,1)S(1)}, u32[]{:S(2)}, u32[]{:S(2)}) collective-permute-start(bf16[64,2048]{1,0:T(8,128)(2,1)} %slice.192), channel_id=1, source_target_pairs={{0,8},{8,16},{16,24},{24,28},{28,20},{20,12},{12,4},{4,0},{1,9},{9... | collective-permute-start | bytes 786440 | tf_op jit(solution)/shard_map/ppermute | solution.py:193
  181.6 11.9 %mix.1 = (bf16[1024,2048]{1,0:T(8,128)(2,1)}, f32[256,2048]{1,0:T(8,128)}) custom-call(s32[1]{0:T(128)} %bitcast.info_ref.block_ref, bf16[1024,128]{1,0:T(8,128)(2,1)} %attend_rest.2.refs_0_, bf16[1024,128]{1,0:T(8,128)(2,1)S(1)} %attend_rest.3.refs_1_, bf16[1024,128]{1,0:T(8,128)(2,1)} %collective-permute-done.8.refs_2_, ...), custom_call_target="tpu_custom_call" | custom-call | flops 4294967296 | bytes 16777216 | tf_op jit(solution)/shard_map/mix/pallas_call | solution.py:244
  195.7 4.5 %acts.4.refs_1_ = bf16[1024,256]{1,0:T(8,128)(2,1)S(1)} custom-call(bf16[1024,2048]{1,0:T(8,128)(2,1)S(1)} %copy-done.2, f32[1024,8]{1,0:T(8,128)S(1)} %copy.66.weight_ref, bf16[2048,256]{1,0:T(8,128)(2,1)} %collective-permute-done.19.refs_0_, bf16[2048,256]{1,0:T(8,128)(2,1)} %collective-permute-done.20.refs_1_), custom_call_target="tpu_custom_call" | custom-call | flops 2147483648 | bytes 6291456 | tf_op jit(solution)/shard_map/acts/pallas_call | solution.py:298
  200.2 5.7 %acts.3.refs_0_ = bf16[1024,384]{1,0:T(8,128)(2,1)S(1)} custom-call(bf16[1024,2048]{1,0:T(8,128)(2,1)S(1)} %copy-done.2, f32[1024,8]{1,0:T(8,128)S(1)} %copy.66.weight_ref, bf16[2048,256]{1,0:T(8,128)(2,1)S(1)} %pad_maximum_fusion.1.refs_0_, bf16[2048,256]{1,0:T(8,128)(2,1)} %collective-permute-done.17.refs_1_, bf16[2048,256]{1,0:T(8,128)(2,1)} %collective-permute-done.18.refs_2_), custom_call_target="tpu_custom_call" | custom-call | flops 3221225472 | bytes 7340032 | tf_op jit(solution)/shard_map/acts/pallas_call | solution.py:298
  210.8 4.5 %acts.5.refs_2_ = bf16[1024,256]{1,0:T(8,128)(2,1)S(1)} custom-call(bf16[1024,2048]{1,0:T(8,128)(2,1)S(1)} %copy-done.2, f32[1024,8]{1,0:T(8,128)S(1)} %copy.66.weight_ref, bf16[2048,256]{1,0:T(8,128)(2,1)} %collective-permute-done.21.refs_0_, bf16[2048,256]{1,0:T(8,128)(2,1)} %collective-permute-done.22.refs_1_), custom_call_target="tpu_custom_call" | custom-call | flops 2147483648 | bytes 6291456 | tf_op jit(solution)/shard_map/acts/pallas_call | solution.py:298
  215.3 7.1 %early.1.early_ref = f32[1024,2048]{1,0:T(8,128)S(1)} custom-call(bf16[1024,384]{1,0:T(8,128)(2,1)S(1)} %acts.3.refs_0_, bf16[1024,256]{1,0:T(8,128)(2,1)S(1)} %acts.4.refs_1_, bf16[1024,256]{1,0:T(8,128)(2,1)S(1)} %acts.5.refs_2_, bf16[128,2048]{1,0:T(8,128)(2,1)S(1)} %dynamic-slice_bitcast_fusion.refs_3_, ...), custom_call_target="tpu_custom_call" | custom-call | flops 3758096384 | bytes 16777216 | tf_op jit(solution)/shard_map/early/pallas_call | solution.py:339
  231.7 22.2 %collective-permute-done.35 = bf16[256,2048]{1,0:T(8,128)(2,1)S(1)} collective-permute-done((bf16[256,2048]{1,0:T(8,128)(2,1)S(1)}, bf16[256,2048]{1,0:T(8,128)(2,1)S(1)}, u32[]{:S(2)}, u32[]{:S(2)}) %collective-permute-start.35) | collective-permute-done | bytes 1048608 | tf_op jit(solution)/shard_map/ppermute | solution.py:193
  (206 shorter events, 72.6 us)
Async XLA Ops:
  4.2 36.8 %collective-permute-start.2 = (bf16[1088,256]{1,0:T(8,128)(2,1)}, bf16[1088,256]{1,0:T(8,128)(2,1)}, u32[]{:S(2)}, u32[]{:S(2)}) collective-permute-start(bf16[1088,256]{1,0:T(8,128)(2,1)} %constant_dynamic-update-slice_fusion), channel_id=1, source_target_pairs={{0,4},{4,8},{8,12},{12,16},{16,20},{20,24},{24,28},{1,5},{5,9},{9,... | collective-permute-start | bytes 1671176 | tf_op jit(solution)/shard_map/ppermute | solution.py:193
  9.9 31.9 %collective-permute-start = (bf16[1088,256]{1,0:T(8,128)(2,1)}, bf16[1088,256]{1,0:T(8,128)(2,1)}, u32[]{:S(2)}, u32[]{:S(2)}) collective-permute-start(bf16[1088,256]{1,0:T(8,128)(2,1)} %constant_dynamic-update-slice_fusion), channel_id=1, source_target_pairs={{0,8},{4,12},{8,16},{12,20},{16,24},{20,28},{1,9},{5,13},{9,17},{1... | collective-permute-start | bytes 1671176 | tf_op jit(solution)/shard_map/ppermute | solution.py:193
  13.4 48.5 %collective-permute-start.4 = (bf16[1024,256]{1,0:T(8,128)(2,1)}, bf16[1024,256]{1,0:T(8,128)(2,1)}, u32[]{:S(2)}, u32[]{:S(2)}) collective-permute-start(bf16[1024,256]{1,0:T(8,128)(2,1)} %refs_0_.3), channel_id=1, source_target_pairs={{0,8},{4,12},{8,16},{12,20},{16,24},{20,28},{1,9},{5,13},{9,17},{1... | collective-permute-start | bytes 1572872 | tf_op jit(solution)/shard_map/ppermute | solution.py:193
  16.9 47.0 %collective-permute-start.6 = (bf16[1024,256]{1,0:T(8,128)(2,1)}, bf16[1024,256]{1,0:T(8,128)(2,1)}, u32[]{:S(2)}, u32[]{:S(2)}) collective-permute-start(bf16[1024,256]{1,0:T(8,128)(2,1)} %refs_0_.3), channel_id=1, source_target_pairs={{0,4},{4,8},{8,12},{12,16},{16,20},{20,24},{24,28},{1,5},{5,9},{9,... | collective-permute-start | bytes 1572872 | tf_op jit(solution)/shard_map/ppermute | solution.py:193
  21.2 45.2 %collective-permute-start.23 = (bf16[128,2048]{1,0:T(8,128)(2,1)S(1)}, bf16[128,2048]{1,0:T(8,128)(2,1)}, u32[]{:S(2)}, u32[]{:S(2)}) collective-permute-start(bf16[128,2048]{1,0:T(8,128)(2,1)S(1)} %dynamic-slice_bitcast_fusion.refs_3_), channel_id=1, source_target_pairs={{0,8},{8,16},{16,24},{24,28},{28,20},{20,12},{12,4},{4,0},{1,9},{9... | collective-permute-start | bytes 1572872 | tf_op jit(solution)/shard_map/ppermute | solution.py:193
  42.6 16.3 %collective-permute-start.3 = (bf16[1088,256]{1,0:T(8,128)(2,1)}, bf16[1088,256]{1,0:T(8,128)(2,1)}, u32[]{:S(2)}, u32[]{:S(2)}) collective-permute-start(bf16[1088,256]{1,0:T(8,128)(2,1)} %collective-permute-done.2.refs_7_), channel_id=1, source_target_pairs={{0,8},{8,16},{16,24},{1,9},{9,17},{17,25},{2,10},{10,18},{18,26},{... | collective-permute-start | bytes 1671176 | tf_op jit(solution)/shard_map/ppermute | solution.py:193
  59.4 39.3 %collective-permute-start.14 = (bf16[256,2176]{1,0:T(8,128)(2,1)S(1)}, bf16[256,2176]{1,0:T(8,128)(2,1)}, u32[]{:S(2)}, u32[]{:S(2)}) collective-permute-start(bf16[256,2176]{1,0:T(8,128)(2,1)S(1)} %pad_maximum_fusion.refs_8_), channel_id=1, source_target_pairs={{0,2},{1,3},{2,0},{3,1},{4,6},{5,7},{6,4},{7,5},{8,10},{9,11},{10,... | collective-permute-start | bytes 3342344 | tf_op jit(solution)/shard_map/ppermute | solution.py:193
  61.9 36.9 %collective-permute-start.17 = (bf16[2048,256]{1,0:T(8,128)(2,1)S(1)}, bf16[2048,256]{1,0:T(8,128)(2,1)}, u32[]{:S(2)}, u32[]{:S(2)}) collective-permute-start(bf16[2048,256]{1,0:T(8,128)(2,1)S(1)} %pad_maximum_fusion.1.refs_0_), channel_id=1, source_target_pairs={{0,8},{8,16},{16,24},{24,28},{28,20},{20,12},{12,4},{4,0},{1,9},{9... | collective-permute-start | bytes 3145736 | tf_op jit(solution)/shard_map/ppermute | solution.py:193
  63.9 17.3 %collective-permute-start.5 = (bf16[1024,256]{1,0:T(8,128)(2,1)}, bf16[1024,256]{1,0:T(8,128)(2,1)S(1)}, u32[]{:S(2)}, u32[]{:S(2)}) collective-permute-start(bf16[1024,256]{1,0:T(8,128)(2,1)} %collective-permute-done.4.refs_2_), channel_id=1, source_target_pairs={{0,4},{8,12},{16,20},{24,28},{1,5},{9,13},{17,21},{25,29},{2,6},{1... | collective-permute-start | bytes 1572872 | tf_op jit(solution)/shard_map/ppermute | solution.py:193
  66.4 29.8 %collective-permute-start.7 = (bf16[1024,256]{1,0:T(8,128)(2,1)}, bf16[1024,256]{1,0:T(8,128)(2,1)}, u32[]{:S(2)}, u32[]{:S(2)}) collective-permute-start(bf16[1024,256]{1,0:T(8,128)(2,1)} %collective-permute-done.6.refs_3_), channel_id=1, source_target_pairs={{0,8},{8,16},{16,24},{1,9},{9,17},{17,25},{2,10},{10,18},{18,26},{... | collective-permute-start | bytes 1572872 | tf_op jit(solution)/shard_map/ppermute | solution.py:193
  72.3 55.3 %collective-permute-start.15 = (bf16[256,2176]{1,0:T(8,128)(2,1)S(1)}, bf16[256,2176]{1,0:T(8,128)(2,1)}, u32[]{:S(2)}, u32[]{:S(2)}) collective-permute-start(bf16[256,2176]{1,0:T(8,128)(2,1)S(1)} %pad_maximum_fusion.refs_8_), channel_id=1, source_target_pairs={{0,1},{1,0},{2,3},{3,2},{4,5},{5,4},{6,7},{7,6},{8,9},{9,8},{10,11... | collective-permute-start | bytes 3342344 | tf_op jit(solution)/shard_map/ppermute | solution.py:193
  82.0 26.1 %collective-permute-start.18 = (bf16[2048,256]{1,0:T(8,128)(2,1)S(1)}, bf16[2048,256]{1,0:T(8,128)(2,1)}, u32[]{:S(2)}, u32[]{:S(2)}) collective-permute-start(bf16[2048,256]{1,0:T(8,128)(2,1)S(1)} %pad_maximum_fusion.1.refs_0_), channel_id=1, source_target_pairs={{8,0},{16,8},{24,16},{28,24},{20,28},{12,20},{4,12},{0,4},{9,1},{1... | collective-permute-start | bytes 3145736 | tf_op jit(solution)/shard_map/ppermute | solution.py:193
  96.3 22.0 %collective-permute-start.25 = (bf16[128,2048]{1,0:T(8,128)(2,1)}, bf16[128,2048]{1,0:T(8,128)(2,1)S(1)}, u32[]{:S(2)}, u32[]{:S(2)}) collective-permute-start(bf16[128,2048]{1,0:T(8,128)(2,1)} %collective-permute-done.23.refs_4_), channel_id=1, source_target_pairs={{0,8},{8,16},{16,24},{24,28},{28,20},{20,12},{12,4},{4,0},{1,9},{9... | collective-permute-start | bytes 1572872 | tf_op jit(solution)/shard_map/ppermute | solution.py:193
  98.7 21.0 %collective-permute-start.26 = (bf16[128,2048]{1,0:T(8,128)(2,1)}, bf16[128,2048]{1,0:T(8,128)(2,1)S(1)}, u32[]{:S(2)}, u32[]{:S(2)}) collective-permute-start(bf16[128,2048]{1,0:T(8,128)(2,1)} %collective-permute-done.24.refs_5_), channel_id=1, source_target_pairs={{8,0},{16,8},{24,16},{28,24},{20,28},{12,20},{4,12},{0,4},{9,1},{1... | collective-permute-start | bytes 1572872 | tf_op jit(solution)/shard_map/ppermute | solution.py:193
  98.8 56.3 %collective-permute-start.16 = (bf16[256,2176]{1,0:T(8,128)(2,1)}, bf16[256,2176]{1,0:T(8,128)(2,1)S(1)}, u32[]{:S(2)}, u32[]{:S(2)}) collective-permute-start(bf16[256,2176]{1,0:T(8,128)(2,1)} %collective-permute-done.14.refs_9_), channel_id=1, source_target_pairs={{0,1},{1,0},{2,3},{3,2},{4,5},{5,4},{6,7},{7,6},{8,9},{9,8},{10,11... | collective-permute-start | bytes 3342344 | tf_op jit(solution)/shard_map/ppermute | solution.py:193
  108.2 59.6 %collective-permute-start.19 = (bf16[2048,256]{1,0:T(8,128)(2,1)}, bf16[2048,256]{1,0:T(8,128)(2,1)}, u32[]{:S(2)}, u32[]{:S(2)}) collective-permute-start(bf16[2048,256]{1,0:T(8,128)(2,1)} %collective-permute-done.17.refs_1_), channel_id=1, source_target_pairs={{0,8},{8,16},{16,24},{24,28},{28,20},{20,12},{12,4},{4,0},{1,9},{9... | collective-permute-start | bytes 3145736 | tf_op jit(solution)/shard_map/ppermute | solution.py:193
  118.2 52.1 %collective-permute-start.20 = (bf16[2048,256]{1,0:T(8,128)(2,1)}, bf16[2048,256]{1,0:T(8,128)(2,1)}, u32[]{:S(2)}, u32[]{:S(2)}) collective-permute-start(bf16[2048,256]{1,0:T(8,128)(2,1)} %collective-permute-done.18.refs_2_), channel_id=1, source_target_pairs={{8,0},{16,8},{24,16},{28,24},{20,28},{12,20},{4,12},{0,4},{9,1},{1... | collective-permute-start | bytes 3145736 | tf_op jit(solution)/shard_map/ppermute | solution.py:193
  119.8 33.0 %collective-permute-start.27 = (bf16[128,2048]{1,0:T(8,128)(2,1)S(1)}, bf16[128,2048]{1,0:T(8,128)(2,1)}, u32[]{:S(2)}, u32[]{:S(2)}) collective-permute-start(bf16[128,2048]{1,0:T(8,128)(2,1)S(1)} %collective-permute-done.25.refs_6_), channel_id=1, source_target_pairs={{0,8},{8,16},{16,24},{24,28},{28,20},{20,12},{12,4},{4,0},{1,9},{9... | collective-permute-start | bytes 1572872 | tf_op jit(solution)/shard_map/ppermute | solution.py:193
  127.6 27.5 %collective-permute-start.28 = (bf16[128,2048]{1,0:T(8,128)(2,1)S(1)}, bf16[128,2048]{1,0:T(8,128)(2,1)}, u32[]{:S(2)}, u32[]{:S(2)}) collective-permute-start(bf16[128,2048]{1,0:T(8,128)(2,1)S(1)} %collective-permute-done.26.refs_7_), channel_id=1, source_target_pairs={{8,0},{16,8},{24,16},{28,24},{20,28},{12,20},{4,12},{0,4},{9,1},{1... | collective-permute-start | bytes 1572872 | tf_op jit(solution)/shard_map/ppermute | solution.py:193
  167.8 38.1 %collective-permute-start.21 = (bf16[2048,256]{1,0:T(8,128)(2,1)}, bf16[2048,256]{1,0:T(8,128)(2,1)}, u32[]{:S(2)}, u32[]{:S(2)}) collective-permute-start(bf16[2048,256]{1,0:T(8,128)(2,1)} %collective-permute-done.19.refs_0_), channel_id=1, source_target_pairs={{0,8},{8,16},{16,24},{24,28},{28,20},{20,12},{12,4},{4,0},{1,9},{9... | collective-permute-start | bytes 3145736 | tf_op jit(solution)/shard_map/ppermute | solution.py:193
  170.4 39.0 %collective-permute-start.22 = (bf16[2048,256]{1,0:T(8,128)(2,1)}, bf16[2048,256]{1,0:T(8,128)(2,1)}, u32[]{:S(2)}, u32[]{:S(2)}) collective-permute-start(bf16[2048,256]{1,0:T(8,128)(2,1)} %collective-permute-done.20.refs_1_), channel_id=1, source_target_pairs={{8,0},{16,8},{24,16},{28,24},{20,28},{12,20},{4,12},{0,4},{9,1},{1... | collective-permute-start | bytes 3145736 | tf_op jit(solution)/shard_map/ppermute | solution.py:193
  170.7 51.7 %collective-permute-start.31 = (bf16[64,2048]{1,0:T(8,128)(2,1)}, bf16[64,2048]{1,0:T(8,128)(2,1)S(1)}, u32[]{:S(2)}, u32[]{:S(2)}) collective-permute-start(bf16[64,2048]{1,0:T(8,128)(2,1)} %slice.192), channel_id=1, source_target_pairs={{0,8},{8,16},{16,24},{24,28},{28,20},{20,12},{12,4},{4,0},{1,9},{9... | collective-permute-start | bytes 786440 | tf_op jit(solution)/shard_map/ppermute | solution.py:193
  180.6 41.8 %collective-permute-start.32 = (bf16[64,2048]{1,0:T(8,128)(2,1)}, bf16[64,2048]{1,0:T(8,128)(2,1)S(1)}, u32[]{:S(2)}, u32[]{:S(2)}) collective-permute-start(bf16[64,2048]{1,0:T(8,128)(2,1)} %slice.193), channel_id=1, source_target_pairs={{8,0},{16,8},{24,16},{28,24},{20,28},{12,20},{4,12},{0,4},{9,1},{1... | collective-permute-start | bytes 786440 | tf_op jit(solution)/shard_map/ppermute | solution.py:193
  228.7 25.1 %collective-permute-start.35 = (bf16[256,2048]{1,0:T(8,128)(2,1)S(1)}, bf16[256,2048]{1,0:T(8,128)(2,1)S(1)}, u32[]{:S(2)}, u32[]{:S(2)}) collective-permute-start(bf16[256,2048]{1,0:T(8,128)(2,1)S(1)} %add_convert_fusion.1), channel_id=1, source_target_pairs={{0,2},{1,3},{2,0},{3,1},{4,6},{5,7},{6,4},{7,5},{8,10},{9,11},{10,... | collective-permute-start | bytes 3145736 | tf_op jit(solution)/shard_map/ppermute | solution.py:193
  (48 other events, 464.2 us)

commit v2 on v1

--- a/solution.py
+++ b/solution.py
@@ -411,17 +411,20 @@
     after = lax.optimization_barrier
     flip = lambda bit: [(i, i ^ bit) for i in range(parts)]
 
-    def behind(x):
-        one = send(x, "sp", [(i, i + 1) for i in range(n - 1)])
+    def behind(x, by_even):
         two = send(x, "sp", [(i, i + 2) for i in range(n - 2)])
-        far = send(one, "sp", [(i, i + 2) for i in range(0, n - 2, 2)])
-        side = send(two, "sp", [(i, i + 1) for i in range(0, n - 1, 2)])
-        return side, far, two, one
-
-    key_blocks = behind(key_rows)
+        one = send(x, "sp", [(i, i + 1) for i in range(0, n - 1, 2)])
+        swap = send(two, "sp", [(i, i ^ 1) for i in range(n)])
+        if by_even:
+            far = send(swap, "sp", [(i, i + 2) for i in range(0, n - 2, 2)])
+        else:
+            far = send(two, "sp", [(i, i + 1) for i in range(1, n - 1, 2)])
+        return swap, far, two, one
+
+    key_blocks = behind(key_rows, True)
     marks = jnp.concatenate([*three_parts(forget_cum), doc_ids[None].astype(jnp.bfloat16)])
     marks = jnp.pad(marks, ((0, 4 * heads - marks.shape[0]), (0, 0))).reshape(-1, width)
-    value_blocks = behind(jnp.concatenate([value_rows, marks], axis=0))
+    value_blocks = behind(jnp.concatenate([value_rows, marks], axis=0), False)
     odd = s % 2 == 1
 
     def expert_at(place):
@@ -488,8 +491,11 @@
                 forget_cum[None] - origin, docs, docs, head_size, None,
             )
         )
-    side, far, two, one = [x[tok:] for x in value_blocks]
-    sent = [x.reshape(-1, tok).astype(jnp.float32) for x in (jnp.where(odd, side, far), two, one)]
+    swap, far, two, one = [x[tok:] for x in value_blocks]
+    sent = [
+        x.reshape(-1, tok).astype(jnp.float32)
+        for x in (jnp.where(odd, swap, far), two, jnp.where(odd, one, swap))
+    ]
     earlier = jnp.concatenate(
         [x[:heads] + x[heads : 2 * heads] + x[2 * heads : 3 * heads] for x in sent], axis=1
     )
@@ -502,8 +508,11 @@
     for p in range(pairs):
         attended.append(
             attend(
-                p, query_rows, [(x, 0, y, 0) for x, y in zip(key_blocks, value_blocks)],
-                (2, 1, 1), pick, bounds, relative, earlier_docs, docs, head_size, states[p],
+                p, query_rows, [
+                    (x, 0, y, 0)
+                    for x, y in zip((*key_blocks, key_blocks[0]), (*value_blocks, value_blocks[0]))
+                ],
+                (2, 1, 2), pick, bounds, relative, earlier_docs, docs, head_size, states[p],
             )
         )
     wide[2] = ring(2, *wide[1])

time: 257 us -> 244 us (0.949)
  waiting for transfers between devices: 79.9 us -> 70.6 us
    ppermute x36, waiting for transfers between devices: 79.9 us -> 70.6 us  [send(): return lax.ppermute(x, axis, pairs)]
    unnamed x77, local copies, waits for them, and re-layouts: 17.3 us -> 14.7 us
  transfers between devices with their start and end apart: 36 -> 36, of which waited for: 11 -> 9; matrix products, arithmetic and copies ran while one was open for 9% -> 9% of each run, Pallas kernels for 21% -> 23%
where the time goes in v2:
time: 244 us; the launch traced here: 243 us
  starting transfers between devices  75.1 us (31%)
  waiting for transfers between devices  70.6 us (29%)
  Pallas kernels  56 us (23%)
  local copies, waits for them, and re-layouts  32.9 us (13%)
  other arithmetic  7.41 us (3%)
    ppermute x36, starting transfers between devices, send(): return lax.ppermute(x, axis, pairs)  75.1 us
    ppermute x36, waiting for transfers between devices, send(): return lax.ppermute(x, axis, pairs)  70.6 us
    pallas_call x4, Pallas kernels, attend(): pl.pallas_call(functools.partial(attend_kernel, sources=sources, own=own,...  17.5 us
    pallas_call x3, Pallas kernels, acts_of(): pl.pallas_call(functools.partial(acts_kernel, first=first), out_shape=jax...  14.9 us
    unnamed x77, local copies, waits for them, and re-layouts  14.7 us
    pallas_call x1, Pallas kernels, mix(): pl.pallas_call(functools.partial(mix_kernel, offsets=offsets, pairs=pairs...  11.5 us
    pallas_call x1, Pallas kernels, early_sums(): pl.pallas_call(functools.partial(early_kernel, groups=len(acts)), out_sha...  6.88 us
    dynamic_update_slice x5, local copies, waits for them, and re-layouts, per_device(): lax.dynamic_update_slice_in_dim(tail, x[:, model:], (t ^ o) * tok_loc, 0)  5.21 us
  transfers between devices with their start and end apart: 36, of which 9 were waited for; matrix products, arithmetic and copies ran while one was open for 9% of the time, Pallas kernels for 23%

profile of v2, /device:TPU:0, one launch (start us, length us, event | category | flops | bytes accessed | tf_op | source)
XLA Modules:
  0.0 243.0 jit_solution(15728757014782563176)
XLA Ops:
  4.2 5.8 %collective-permute-start = (bf16[1088,256]{1,0:T(8,128)(2,1)}, bf16[1088,256]{1,0:T(8,128)(2,1)}, u32[]{:S(2)}, u32[]{:S(2)}) collective-permute-start(bf16[1088,256]{1,0:T(8,128)(2,1)} %constant_dynamic-update-slice_fusion), channel_id=1, source_target_pairs={{0,8},{4,12},{8,16},{12,20},{16,24},{20,28},{1,9},{5,13},{9,17},{1... | collective-permute-start | bytes 1671176 | tf_op jit(solution)/shard_map/ppermute | solution.py:193
  10.0 4.2 %collective-permute-start.3 = (bf16[1088,256]{1,0:T(8,128)(2,1)}, bf16[1088,256]{1,0:T(8,128)(2,1)}, u32[]{:S(2)}, u32[]{:S(2)}) collective-permute-start(bf16[1088,256]{1,0:T(8,128)(2,1)} %constant_dynamic-update-slice_fusion), channel_id=1, source_target_pairs={{0,4},{8,12},{16,20},{24,28},{1,5},{9,13},{17,21},{25,29},{2,6},{1... | collective-permute-start | bytes 1671176 | tf_op jit(solution)/shard_map/ppermute | solution.py:193
  14.2 3.5 %collective-permute-start.4 = (bf16[1024,256]{1,0:T(8,128)(2,1)}, bf16[1024,256]{1,0:T(8,128)(2,1)}, u32[]{:S(2)}, u32[]{:S(2)}) collective-permute-start(bf16[1024,256]{1,0:T(8,128)(2,1)} %refs_0_.3), channel_id=1, source_target_pairs={{0,8},{4,12},{8,16},{12,20},{16,24},{20,28},{1,9},{5,13},{9,17},{1... | collective-permute-start | bytes 1572872 | tf_op jit(solution)/shard_map/ppermute | solution.py:193
  25.7 5.2 %attend_own.2 = (f32[1024,128]{1,0:T(8,128)S(1)}, f32[1024,128]{1,0:T(8,128)S(1)}, f32[1024,128]{1,0:T(8,128)S(1)}) custom-call(s32[2]{0:T(128)S(1)} %get-tuple-element.30.low_ref, s32[2]{0:T(128)S(1)} %get-tuple-element.29.full_ref, s32[1]{0:T(128)} %bitcast.1.pick_ref, bf16[1024,256]{1,0:T(8,128)(2,1)S(1)} %copy-done.12, bf16[1024,256]{1,0:T(8,128)(2,1)S(1)} %copy-done.11, ...), custom_call_target="tpu_custom_call" | custom-call | flops 2147483648 | bytes 1572864 | tf_op jit(solution)/shard_map/attend_own/pallas_call | solution.py:150
  33.3 5.2 %attend_own.3 = (f32[1024,128]{1,0:T(8,128)S(1)}, f32[1024,128]{1,0:T(8,128)S(1)}, f32[1024,128]{1,0:T(8,128)S(1)}) custom-call(s32[2]{0:T(128)S(1)} %get-tuple-element.30.low_ref, s32[2]{0:T(128)S(1)} %get-tuple-element.29.full_ref, s32[1]{0:T(128)} %bitcast.1.pick_ref, bf16[1024,256]{1,0:T(8,128)(2,1)S(1)} %copy-done.12, bf16[1024,256]{1,0:T(8,128)(2,1)S(1)} %copy-done.11, ...), custom_call_target="tpu_custom_call" | custom-call | flops 2147483648 | bytes 1572864 | tf_op jit(solution)/shard_map/attend_own/pallas_call | solution.py:150
  42.6 3.5 %collective-permute-start.1 = (bf16[1088,256]{1,0:T(8,128)(2,1)}, bf16[1088,256]{1,0:T(8,128)(2,1)}, u32[]{:S(2)}, u32[]{:S(2)}) collective-permute-start(bf16[1088,256]{1,0:T(8,128)(2,1)} %collective-permute-done.refs_7_), channel_id=1, source_target_pairs={{0,4},{4,0},{8,12},{12,8},{16,20},{20,16},{24,28},{28,24},{1,5},{5... | collective-permute-start | bytes 1671176 | tf_op jit(solution)/shard_map/ppermute | solution.py:193
  50.6 9.3 %collective-permute-done.1.refs_5_.refs_9_ = bf16[1088,256]{1,0:T(8,128)(2,1)} collective-permute-done((bf16[1088,256]{1,0:T(8,128)(2,1)}, bf16[1088,256]{1,0:T(8,128)(2,1)}, u32[]{:S(2)}, u32[]{:S(2)}) %collective-permute-start.1) | collective-permute-done | bytes 557088 | tf_op jit(solution)/shard_map/ppermute | solution.py:193
  63.0 8.3 %collective-permute-start.17 = (bf16[2048,256]{1,0:T(8,128)(2,1)S(1)}, bf16[2048,256]{1,0:T(8,128)(2,1)}, u32[]{:S(2)}, u32[]{:S(2)}) collective-permute-start(bf16[2048,256]{1,0:T(8,128)(2,1)S(1)} %pad_maximum_fusion.1.refs_0_), channel_id=1, source_target_pairs={{0,8},{8,16},{16,24},{24,28},{28,20},{20,12},{12,4},{4,0},{1,9},{9... | collective-permute-start | bytes 3145736 | tf_op jit(solution)/shard_map/ppermute | solution.py:193
  73.6 7.9 %collective-permute-start.18 = (bf16[2048,256]{1,0:T(8,128)(2,1)S(1)}, bf16[2048,256]{1,0:T(8,128)(2,1)}, u32[]{:S(2)}, u32[]{:S(2)}) collective-permute-start(bf16[2048,256]{1,0:T(8,128)(2,1)S(1)} %pad_maximum_fusion.1.refs_0_), channel_id=1, source_target_pairs={{8,0},{16,8},{24,16},{28,24},{20,28},{12,20},{4,12},{0,4},{9,1},{1... | collective-permute-start | bytes 3145736 | tf_op jit(solution)/shard_map/ppermute | solution.py:193
  85.4 3.9 %collective-permute-start.6 = (bf16[1024,256]{1,0:T(8,128)(2,1)}, bf16[1024,256]{1,0:T(8,128)(2,1)S(1)}, u32[]{:S(2)}, u32[]{:S(2)}) collective-permute-start(bf16[1024,256]{1,0:T(8,128)(2,1)} %collective-permute-done.5.refs_0_.refs_4_), channel_id=1, source_target_pairs={{0,8},{8,16},{16,24},{1,9},{9,17},{17,25},{2,10},{10,18},{18,26},{... | collective-permute-start | bytes 1572872 | tf_op jit(solution)/shard_map/ppermute | solution.py:193
  89.4 15.5 %collective-permute-done.17.refs_1_ = bf16[2048,256]{1,0:T(8,128)(2,1)} collective-permute-done((bf16[2048,256]{1,0:T(8,128)(2,1)S(1)}, bf16[2048,256]{1,0:T(8,128)(2,1)}, u32[]{:S(2)}, u32[]{:S(2)}) %collective-permute-start.17) | collective-permute-done | bytes 1048608 | tf_op jit(solution)/shard_map/ppermute | solution.py:193
  104.9 4.7 %collective-permute-start.19 = (bf16[2048,256]{1,0:T(8,128)(2,1)}, bf16[2048,256]{1,0:T(8,128)(2,1)}, u32[]{:S(2)}, u32[]{:S(2)}) collective-permute-start(bf16[2048,256]{1,0:T(8,128)(2,1)} %collective-permute-done.17.refs_1_), channel_id=1, source_target_pairs={{0,8},{8,16},{16,24},{24,28},{28,20},{20,12},{12,4},{4,0},{1,9},{9... | collective-permute-start | bytes 3145736 | tf_op jit(solution)/shard_map/ppermute | solution.py:193
  109.5 6.5 %collective-permute-done.25.refs_6_ = bf16[128,2048]{1,0:T(8,128)(2,1)S(1)} collective-permute-done((bf16[128,2048]{1,0:T(8,128)(2,1)}, bf16[128,2048]{1,0:T(8,128)(2,1)S(1)}, u32[]{:S(2)}, u32[]{:S(2)}) %collective-permute-start.25) | collective-permute-done | bytes 524320 | tf_op jit(solution)/shard_map/ppermute | solution.py:193
  121.6 3.2 %attend_rest.2.refs_0_ = bf16[1024,128]{1,0:T(8,128)(2,1)S(1)} custom-call(s32[2]{0:T(128)S(1)} %get-tuple-element.47.low_ref, s32[2]{0:T(128)S(1)} %get-tuple-element.48.full_ref, s32[1]{0:T(128)} %bitcast.1.pick_ref, bf16[1024,256]{1,0:T(8,128)(2,1)S(1)} %copy-done.13, bf16[1024,256]{1,0:T(8,128)(2,1)} %collective-permute-done.5.refs_0_.refs_4_, ...), custom_call_target="tpu_custom_call" | custom-call | flops 6442450944 | bytes 1572864 | tf_op jit(solution)/shard_map/attend_rest/pallas_call | solution.py:150
  124.9 10.9 %collective-permute-start.27 = (bf16[128,2048]{1,0:T(8,128)(2,1)S(1)}, bf16[128,2048]{1,0:T(8,128)(2,1)S(1)}, u32[]{:S(2)}, u32[]{:S(2)}) collective-permute-start(bf16[128,2048]{1,0:T(8,128)(2,1)S(1)} %collective-permute-done.25.refs_6_), channel_id=1, source_target_pairs={{0,8},{8,16},{16,24},{24,28},{28,20},{20,12},{12,4},{4,0},{1,9},{9... | collective-permute-start | bytes 1572872 | tf_op jit(solution)/shard_map/ppermute | solution.py:193
  135.8 3.9 %attend_rest.3.refs_1_ = bf16[1024,128]{1,0:T(8,128)(2,1)} custom-call(s32[2]{0:T(128)S(1)} %get-tuple-element.47.low_ref, s32[2]{0:T(128)S(1)} %get-tuple-element.48.full_ref, s32[1]{0:T(128)} %bitcast.1.pick_ref, bf16[1024,256]{1,0:T(8,128)(2,1)S(1)} %copy-done.13, bf16[1024,256]{1,0:T(8,128)(2,1)} %collective-permute-done.5.refs_0_.refs_4_, ...), custom_call_target="tpu_custom_call" | custom-call | flops 6442450944 | bytes 1572864 | tf_op jit(solution)/shard_map/attend_rest/pallas_call | solution.py:150
  139.8 10.0 %collective-permute-done.27.refs_8_ = bf16[128,2048]{1,0:T(8,128)(2,1)S(1)} collective-permute-done((bf16[128,2048]{1,0:T(8,128)(2,1)S(1)}, bf16[128,2048]{1,0:T(8,128)(2,1)S(1)}, u32[]{:S(2)}, u32[]{:S(2)}) %collective-permute-start.27) | collective-permute-done | bytes 524320 | tf_op jit(solution)/shard_map/ppermute | solution.py:193
  163.0 2.5 %collective-permute-start.21 = (bf16[2048,256]{1,0:T(8,128)(2,1)}, bf16[2048,256]{1,0:T(8,128)(2,1)}, u32[]{:S(2)}, u32[]{:S(2)}) collective-permute-start(bf16[2048,256]{1,0:T(8,128)(2,1)} %collective-permute-done.19.refs_0_), channel_id=1, source_target_pairs={{0,8},{8,16},{16,24},{24,28},{28,20},{20,12},{12,4},{4,0},{1,9},{9... | collective-permute-start | bytes 3145736 | tf_op jit(solution)/shard_map/ppermute | solution.py:193
  169.8 11.5 %mix.1 = (bf16[1024,2048]{1,0:T(8,128)(2,1)}, f32[256,2048]{1,0:T(8,128)}) custom-call(s32[1]{0:T(128)} %bitcast.info_ref.block_ref, bf16[1024,128]{1,0:T(8,128)(2,1)S(1)} %attend_rest.2.refs_0_, bf16[1024,128]{1,0:T(8,128)(2,1)} %attend_rest.3.refs_1_, bf16[1024,128]{1,0:T(8,128)(2,1)S(1)} %collective-permute-done.8.refs_2_, ...), custom_call_target="tpu_custom_call" | custom-call | flops 4294967296 | bytes 16777216 | tf_op jit(solution)/shard_map/mix/pallas_call | solution.py:244
  183.6 4.5 %acts.4.refs_1_ = bf16[1024,256]{1,0:T(8,128)(2,1)S(1)} custom-call(bf16[1024,2048]{1,0:T(8,128)(2,1)S(1)} %copy-done.2, f32[1024,8]{1,0:T(8,128)S(1)} %copy.66.weight_ref, bf16[2048,256]{1,0:T(8,128)(2,1)} %collective-permute-done.19.refs_0_, bf16[2048,256]{1,0:T(8,128)(2,1)} %collective-permute-done.20.refs_1_), custom_call_target="tpu_custom_call" | custom-call | flops 2147483648 | bytes 6291456 | tf_op jit(solution)/shard_map/acts/pallas_call | solution.py:298
  188.1 5.6 %acts.3.refs_0_ = bf16[1024,384]{1,0:T(8,128)(2,1)S(1)} custom-call(bf16[1024,2048]{1,0:T(8,128)(2,1)S(1)} %copy-done.2, f32[1024,8]{1,0:T(8,128)S(1)} %copy.66.weight_ref, bf16[2048,256]{1,0:T(8,128)(2,1)S(1)} %pad_maximum_fusion.1.refs_0_, bf16[2048,256]{1,0:T(8,128)(2,1)} %collective-permute-done.17.refs_1_, bf16[2048,256]{1,0:T(8,128)(2,1)} %collective-permute-done.18.refs_2_), custom_call_target="tpu_custom_call" | custom-call | flops 3221225472 | bytes 7340032 | tf_op jit(solution)/shard_map/acts/pallas_call | solution.py:298
  198.4 4.7 %acts.5.refs_2_ = bf16[1024,256]{1,0:T(8,128)(2,1)S(1)} custom-call(bf16[1024,2048]{1,0:T(8,128)(2,1)S(1)} %copy-done.2, f32[1024,8]{1,0:T(8,128)S(1)} %copy.66.weight_ref, bf16[2048,256]{1,0:T(8,128)(2,1)} %collective-permute-done.21.refs_0_, bf16[2048,256]{1,0:T(8,128)(2,1)} %collective-permute-done.22.refs_1_), custom_call_target="tpu_custom_call" | custom-call | flops 2147483648 | bytes 6291456 | tf_op jit(solution)/shard_map/acts/pallas_call | solution.py:298
  203.1 6.9 %early.1.early_ref = f32[1024,2048]{1,0:T(8,128)S(1)} custom-call(bf16[1024,384]{1,0:T(8,128)(2,1)S(1)} %acts.3.refs_0_, bf16[1024,256]{1,0:T(8,128)(2,1)S(1)} %acts.4.refs_1_, bf16[1024,256]{1,0:T(8,128)(2,1)S(1)} %acts.5.refs_2_, bf16[128,2048]{1,0:T(8,128)(2,1)S(1)} %copy-done.6, bf16[128,2048]{1,0:T(8,128)(2,1)} %collective-permute-done.23.refs_4_, ...), custom_call_target="tpu_custom_call" | custom-call | flops 3758096384 | bytes 16777216 | tf_op jit(solution)/shard_map/early/pallas_call | solution.py:339
  219.2 22.5 %collective-permute-done.35 = bf16[256,2048]{1,0:T(8,128)(2,1)S(1)} collective-permute-done((bf16[256,2048]{1,0:T(8,128)(2,1)S(1)}, bf16[256,2048]{1,0:T(8,128)(2,1)S(1)}, u32[]{:S(2)}, u32[]{:S(2)}) %collective-permute-start.35) | collective-permute-done | bytes 1048608 | tf_op jit(solution)/shard_map/ppermute | solution.py:193
  (204 shorter events, 72.3 us)
Async XLA Ops:
  4.2 36.8 %collective-permute-start = (bf16[1088,256]{1,0:T(8,128)(2,1)}, bf16[1088,256]{1,0:T(8,128)(2,1)}, u32[]{:S(2)}, u32[]{:S(2)}) collective-permute-start(bf16[1088,256]{1,0:T(8,128)(2,1)} %constant_dynamic-update-slice_fusion), channel_id=1, source_target_pairs={{0,8},{4,12},{8,16},{12,20},{16,24},{20,28},{1,9},{5,13},{9,17},{1... | collective-permute-start | bytes 1671176 | tf_op jit(solution)/shard_map/ppermute | solution.py:193
  10.0 37.1 %collective-permute-start.3 = (bf16[1088,256]{1,0:T(8,128)(2,1)}, bf16[1088,256]{1,0:T(8,128)(2,1)}, u32[]{:S(2)}, u32[]{:S(2)}) collective-permute-start(bf16[1088,256]{1,0:T(8,128)(2,1)} %constant_dynamic-update-slice_fusion), channel_id=1, source_target_pairs={{0,4},{8,12},{16,20},{24,28},{1,5},{9,13},{17,21},{25,29},{2,6},{1... | collective-permute-start | bytes 1671176 | tf_op jit(solution)/shard_map/ppermute | solution.py:193
  14.2 32.8 %collective-permute-start.4 = (bf16[1024,256]{1,0:T(8,128)(2,1)}, bf16[1024,256]{1,0:T(8,128)(2,1)}, u32[]{:S(2)}, u32[]{:S(2)}) collective-permute-start(bf16[1024,256]{1,0:T(8,128)(2,1)} %refs_0_.3), channel_id=1, source_target_pairs={{0,8},{4,12},{8,16},{12,20},{16,24},{20,28},{1,9},{5,13},{9,17},{1... | collective-permute-start | bytes 1572872 | tf_op jit(solution)/shard_map/ppermute | solution.py:193
  17.7 45.3 %collective-permute-start.7 = (bf16[1024,256]{1,0:T(8,128)(2,1)}, bf16[1024,256]{1,0:T(8,128)(2,1)}, u32[]{:S(2)}, u32[]{:S(2)}) collective-permute-start(bf16[1024,256]{1,0:T(8,128)(2,1)} %refs_0_.3), channel_id=1, source_target_pairs={{0,4},{8,12},{16,20},{24,28},{1,5},{9,13},{17,21},{25,29},{2,6},{1... | collective-permute-start | bytes 1572872 | tf_op jit(solution)/shard_map/ppermute | solution.py:193
  42.6 17.3 %collective-permute-start.1 = (bf16[1088,256]{1,0:T(8,128)(2,1)}, bf16[1088,256]{1,0:T(8,128)(2,1)}, u32[]{:S(2)}, u32[]{:S(2)}) collective-permute-start(bf16[1088,256]{1,0:T(8,128)(2,1)} %collective-permute-done.refs_7_), channel_id=1, source_target_pairs={{0,4},{4,0},{8,12},{12,8},{16,20},{20,16},{24,28},{28,24},{1,5},{5... | collective-permute-start | bytes 1671176 | tf_op jit(solution)/shard_map/ppermute | solution.py:193
  47.0 36.4 %collective-permute-start.23 = (bf16[128,2048]{1,0:T(8,128)(2,1)S(1)}, bf16[128,2048]{1,0:T(8,128)(2,1)}, u32[]{:S(2)}, u32[]{:S(2)}) collective-permute-start(bf16[128,2048]{1,0:T(8,128)(2,1)S(1)} %copy-done.5), channel_id=1, source_target_pairs={{0,8},{8,16},{16,24},{24,28},{28,20},{20,12},{12,4},{4,0},{1,9},{9... | collective-permute-start | bytes 1572872 | tf_op jit(solution)/shard_map/ppermute | solution.py:193
  47.1 36.3 %collective-permute-start.24 = (bf16[128,2048]{1,0:T(8,128)(2,1)S(1)}, bf16[128,2048]{1,0:T(8,128)(2,1)}, u32[]{:S(2)}, u32[]{:S(2)}) collective-permute-start(bf16[128,2048]{1,0:T(8,128)(2,1)S(1)} %copy-done.5), channel_id=1, source_target_pairs={{8,0},{16,8},{24,16},{28,24},{20,28},{12,20},{4,12},{0,4},{9,1},{1... | collective-permute-start | bytes 1572872 | tf_op jit(solution)/shard_map/ppermute | solution.py:193
  49.1 24.4 %collective-permute-start.14 = (bf16[256,2176]{1,0:T(8,128)(2,1)S(1)}, bf16[256,2176]{1,0:T(8,128)(2,1)}, u32[]{:S(2)}, u32[]{:S(2)}) collective-permute-start(bf16[256,2176]{1,0:T(8,128)(2,1)S(1)} %pad_maximum_fusion.refs_8_), channel_id=1, source_target_pairs={{0,2},{1,3},{2,0},{3,1},{4,6},{5,7},{6,4},{7,5},{8,10},{9,11},{10,... | collective-permute-start | bytes 3342344 | tf_op jit(solution)/shard_map/ppermute | solution.py:193
  59.9 25.4 %collective-permute-start.5 = (bf16[1024,256]{1,0:T(8,128)(2,1)}, bf16[1024,256]{1,0:T(8,128)(2,1)}, u32[]{:S(2)}, u32[]{:S(2)}) collective-permute-start(bf16[1024,256]{1,0:T(8,128)(2,1)} %collective-permute-done.4.refs_2_), channel_id=1, source_target_pairs={{0,4},{4,0},{8,12},{12,8},{16,20},{20,16},{24,28},{28,24},{1,5},{5... | collective-permute-start | bytes 1572872 | tf_op jit(solution)/shard_map/ppermute | solution.py:193
  63.0 41.9 %collective-permute-start.17 = (bf16[2048,256]{1,0:T(8,128)(2,1)S(1)}, bf16[2048,256]{1,0:T(8,128)(2,1)}, u32[]{:S(2)}, u32[]{:S(2)}) collective-permute-start(bf16[2048,256]{1,0:T(8,128)(2,1)S(1)} %pad_maximum_fusion.1.refs_0_), channel_id=1, source_target_pairs={{0,8},{8,16},{16,24},{24,28},{28,20},{20,12},{12,4},{4,0},{1,9},{9... | collective-permute-start | bytes 3145736 | tf_op jit(solution)/shard_map/ppermute | solution.py:193
  73.6 31.3 %collective-permute-start.18 = (bf16[2048,256]{1,0:T(8,128)(2,1)S(1)}, bf16[2048,256]{1,0:T(8,128)(2,1)}, u32[]{:S(2)}, u32[]{:S(2)}) collective-permute-start(bf16[2048,256]{1,0:T(8,128)(2,1)S(1)} %pad_maximum_fusion.1.refs_0_), channel_id=1, source_target_pairs={{8,0},{16,8},{24,16},{28,24},{20,28},{12,20},{4,12},{0,4},{9,1},{1... | collective-permute-start | bytes 3145736 | tf_op jit(solution)/shard_map/ppermute | solution.py:193
  83.4 52.4 %collective-permute-start.15 = (bf16[256,2176]{1,0:T(8,128)(2,1)S(1)}, bf16[256,2176]{1,0:T(8,128)(2,1)S(1)}, u32[]{:S(2)}, u32[]{:S(2)}) collective-permute-start(bf16[256,2176]{1,0:T(8,128)(2,1)S(1)} %pad_maximum_fusion.refs_8_), channel_id=1, source_target_pairs={{0,1},{1,0},{2,3},{3,2},{4,5},{5,4},{6,7},{7,6},{8,9},{9,8},{10,11... | collective-permute-start | bytes 3342344 | tf_op jit(solution)/shard_map/ppermute | solution.py:193
  83.4 32.6 %collective-permute-start.25 = (bf16[128,2048]{1,0:T(8,128)(2,1)}, bf16[128,2048]{1,0:T(8,128)(2,1)S(1)}, u32[]{:S(2)}, u32[]{:S(2)}) collective-permute-start(bf16[128,2048]{1,0:T(8,128)(2,1)} %collective-permute-done.23.refs_4_), channel_id=1, source_target_pairs={{0,8},{8,16},{16,24},{24,28},{28,20},{20,12},{12,4},{4,0},{1,9},{9... | collective-permute-start | bytes 1572872 | tf_op jit(solution)/shard_map/ppermute | solution.py:193
  85.4 32.0 %collective-permute-start.6 = (bf16[1024,256]{1,0:T(8,128)(2,1)}, bf16[1024,256]{1,0:T(8,128)(2,1)S(1)}, u32[]{:S(2)}, u32[]{:S(2)}) collective-permute-start(bf16[1024,256]{1,0:T(8,128)(2,1)} %collective-permute-done.5.refs_0_.refs_4_), channel_id=1, source_target_pairs={{0,8},{8,16},{16,24},{1,9},{9,17},{17,25},{2,10},{10,18},{18,26},{... | collective-permute-start | bytes 1572872 | tf_op jit(solution)/shard_map/ppermute | solution.py:193
  104.9 20.0 %collective-permute-start.26 = (bf16[128,2048]{1,0:T(8,128)(2,1)}, bf16[128,2048]{1,0:T(8,128)(2,1)S(1)}, u32[]{:S(2)}, u32[]{:S(2)}) collective-permute-start(bf16[128,2048]{1,0:T(8,128)(2,1)} %collective-permute-done.24.refs_5_), channel_id=1, source_target_pairs={{8,0},{16,8},{24,16},{28,24},{20,28},{12,20},{4,12},{0,4},{9,1},{1... | collective-permute-start | bytes 1572872 | tf_op jit(solution)/shard_map/ppermute | solution.py:193
  104.9 58.1 %collective-permute-start.19 = (bf16[2048,256]{1,0:T(8,128)(2,1)}, bf16[2048,256]{1,0:T(8,128)(2,1)}, u32[]{:S(2)}, u32[]{:S(2)}) collective-permute-start(bf16[2048,256]{1,0:T(8,128)(2,1)} %collective-permute-done.17.refs_1_), channel_id=1, source_target_pairs={{0,8},{8,16},{16,24},{24,28},{28,20},{20,12},{12,4},{4,0},{1,9},{9... | collective-permute-start | bytes 3145736 | tf_op jit(solution)/shard_map/ppermute | solution.py:193
  116.0 49.5 %collective-permute-start.20 = (bf16[2048,256]{1,0:T(8,128)(2,1)}, bf16[2048,256]{1,0:T(8,128)(2,1)}, u32[]{:S(2)}, u32[]{:S(2)}) collective-permute-start(bf16[2048,256]{1,0:T(8,128)(2,1)} %collective-permute-done.18.refs_2_), channel_id=1, source_target_pairs={{8,0},{16,8},{24,16},{28,24},{20,28},{12,20},{4,12},{0,4},{9,1},{1... | collective-permute-start | bytes 3145736 | tf_op jit(solution)/shard_map/ppermute | solution.py:193
  117.4 33.8 %collective-permute-start.16 = (bf16[256,2176]{1,0:T(8,128)(2,1)}, bf16[256,2176]{1,0:T(8,128)(2,1)}, u32[]{:S(2)}, u32[]{:S(2)}) collective-permute-start(bf16[256,2176]{1,0:T(8,128)(2,1)} %collective-permute-done.14.refs_9_), channel_id=1, source_target_pairs={{0,1},{1,0},{2,3},{3,2},{4,5},{5,4},{6,7},{7,6},{8,9},{9,8},{10,11... | collective-permute-start | bytes 3342344 | tf_op jit(solution)/shard_map/ppermute | solution.py:193
  124.9 24.8 %collective-permute-start.27 = (bf16[128,2048]{1,0:T(8,128)(2,1)S(1)}, bf16[128,2048]{1,0:T(8,128)(2,1)S(1)}, u32[]{:S(2)}, u32[]{:S(2)}) collective-permute-start(bf16[128,2048]{1,0:T(8,128)(2,1)S(1)} %collective-permute-done.25.refs_6_), channel_id=1, source_target_pairs={{0,8},{8,16},{16,24},{24,28},{28,20},{20,12},{12,4},{4,0},{1,9},{9... | collective-permute-start | bytes 1572872 | tf_op jit(solution)/shard_map/ppermute | solution.py:193
  163.0 30.8 %collective-permute-start.21 = (bf16[2048,256]{1,0:T(8,128)(2,1)}, bf16[2048,256]{1,0:T(8,128)(2,1)}, u32[]{:S(2)}, u32[]{:S(2)}) collective-permute-start(bf16[2048,256]{1,0:T(8,128)(2,1)} %collective-permute-done.19.refs_0_), channel_id=1, source_target_pairs={{0,8},{8,16},{16,24},{24,28},{28,20},{20,12},{12,4},{4,0},{1,9},{9... | collective-permute-start | bytes 3145736 | tf_op jit(solution)/shard_map/ppermute | solution.py:193
  165.5 31.5 %collective-permute-start.22 = (bf16[2048,256]{1,0:T(8,128)(2,1)}, bf16[2048,256]{1,0:T(8,128)(2,1)}, u32[]{:S(2)}, u32[]{:S(2)}) collective-permute-start(bf16[2048,256]{1,0:T(8,128)(2,1)} %collective-permute-done.20.refs_1_), channel_id=1, source_target_pairs={{8,0},{16,8},{24,16},{28,24},{20,28},{12,20},{4,12},{0,4},{9,1},{1... | collective-permute-start | bytes 3145736 | tf_op jit(solution)/shard_map/ppermute | solution.py:193
  166.5 43.5 %collective-permute-start.31 = (bf16[64,2048]{1,0:T(8,128)(2,1)}, bf16[64,2048]{1,0:T(8,128)(2,1)S(1)}, u32[]{:S(2)}, u32[]{:S(2)}) collective-permute-start(bf16[64,2048]{1,0:T(8,128)(2,1)} %slice.192), channel_id=1, source_target_pairs={{0,8},{8,16},{16,24},{24,28},{28,20},{20,12},{12,4},{4,0},{1,9},{9... | collective-permute-start | bytes 786440 | tf_op jit(solution)/shard_map/ppermute | solution.py:193
  168.6 41.5 %collective-permute-start.32 = (bf16[64,2048]{1,0:T(8,128)(2,1)}, bf16[64,2048]{1,0:T(8,128)(2,1)S(1)}, u32[]{:S(2)}, u32[]{:S(2)}) collective-permute-start(bf16[64,2048]{1,0:T(8,128)(2,1)} %slice.193), channel_id=1, source_target_pairs={{8,0},{16,8},{24,16},{28,24},{20,28},{12,20},{4,12},{0,4},{9,1},{1... | collective-permute-start | bytes 786440 | tf_op jit(solution)/shard_map/ppermute | solution.py:193
  216.6 25.1 %collective-permute-start.35 = (bf16[256,2048]{1,0:T(8,128)(2,1)S(1)}, bf16[256,2048]{1,0:T(8,128)(2,1)S(1)}, u32[]{:S(2)}, u32[]{:S(2)}) collective-permute-start(bf16[256,2048]{1,0:T(8,128)(2,1)S(1)} %add_convert_fusion.1), channel_id=1, source_target_pairs={{0,2},{1,3},{2,0},{3,1},{4,6},{5,7},{6,4},{7,5},{8,10},{9,11},{10,... | collective-permute-start | bytes 3145736 | tf_op jit(solution)/shard_map/ppermute | solution.py:193
  (48 other events, 414.8 us)

commit v3 on v2

--- a/solution.py
+++ b/solution.py
@@ -330,7 +330,7 @@
     for c in range(0, out_ref.shape[1], chunk):
         out_ref[:, c : c + chunk] = jnp.dot(
             rows, down_all[:, c : c + chunk], preferred_element_type=jnp.float32
-        )
+        ).astype(out_ref.dtype)
 
 
 def early_sums(acts, downs):
@@ -338,7 +338,7 @@
     rows = min(256, tok)
     return pl.pallas_call(
         functools.partial(early_kernel, groups=len(acts)),
-        out_shape=jax.ShapeDtypeStruct((tok, model), jnp.float32),
+        out_shape=jax.ShapeDtypeStruct((tok, model), jnp.bfloat16),
         grid=(tok // rows,),
         in_specs=[pl.BlockSpec((rows, x.shape[1]), lambda i: (i, 0)) for x in acts]
         + [pl.BlockSpec(x.shape, lambda i: (0, 0)) for x in downs],
@@ -356,7 +356,8 @@
     wide, flat, out_ref = refs[:halves], refs[halves:-1], refs[-1]
     act = act_block(x_ref[...], wide, weight_ref[:, at : at + 1])
     lower = jnp.concatenate([x[...] for x in flat], axis=0)
-    total = early_ref[...] + jnp.dot(act, lower, preferred_element_type=jnp.float32)
+    total = jnp.dot(act, lower, preferred_element_type=jnp.float32)
+    total = total + early_ref[...].astype(jnp.float32)
     out_ref[...] = total.astype(out_ref.dtype)
 
 

time: 244 us -> 244 us (level)
  transfers between devices with their start and end apart: 36 -> 36, of which waited for: 9 -> 9; matrix products, arithmetic and copies ran while one was open for 9% -> 9% of each run, Pallas kernels for 23% -> 22%
where the time goes in v3:
time: 244 us; the launch traced here: 243 us
  starting transfers between devices  75.1 us (31%)
  waiting for transfers between devices  70.7 us (29%)
  Pallas kernels  56 us (23%)
  local copies, waits for them, and re-layouts  32.9 us (13%)
  other arithmetic  7.44 us (3%)
    ppermute x36, starting transfers between devices, send(): return lax.ppermute(x, axis, pairs)  75.1 us
    ppermute x36, waiting for transfers between devices, send(): return lax.ppermute(x, axis, pairs)  70.7 us
    pallas_call x4, Pallas kernels, attend(): pl.pallas_call(functools.partial(attend_kernel, sources=sources, own=own,...  17.5 us
    pallas_call x3, Pallas kernels, acts_of(): pl.pallas_call(functools.partial(acts_kernel, first=first), out_shape=jax...  14.9 us
    unnamed x77, local copies, waits for them, and re-layouts  14.7 us
    pallas_call x1, Pallas kernels, mix(): pl.pallas_call(functools.partial(mix_kernel, offsets=offsets, pairs=pairs...  11.5 us
    pallas_call x1, Pallas kernels, early_sums(): pl.pallas_call(functools.partial(early_kernel, groups=len(acts)), out_sha...  6.83 us
    pallas_call x4, Pallas kernels, last_sums(): pl.pallas_call(functools.partial(last_kernel, at=at, halves=len(wide)), o...  5.22 us
  transfers between devices with their start and end apart: 36, of which 9 were waited for; matrix products, arithmetic and copies ran while one was open for 9% of the time, Pallas kernels for 22%

profile of v3, /device:TPU:0, one launch (start us, length us, event | category | flops | bytes accessed | tf_op | source)
XLA Modules:
  0.0 243.0 jit_solution(8244930909307795473)
XLA Ops:
  4.2 5.8 %collective-permute-start = (bf16[1088,256]{1,0:T(8,128)(2,1)}, bf16[1088,256]{1,0:T(8,128)(2,1)}, u32[]{:S(2)}, u32[]{:S(2)}) collective-permute-start(bf16[1088,256]{1,0:T(8,128)(2,1)} %constant_dynamic-update-slice_fusion), channel_id=1, source_target_pairs={{0,8},{4,12},{8,16},{12,20},{16,24},{20,28},{1,9},{5,13},{9,17},{1... | collective-permute-start | bytes 1671176 | tf_op jit(solution)/shard_map/ppermute | solution.py:193
  10.0 4.2 %collective-permute-start.3 = (bf16[1088,256]{1,0:T(8,128)(2,1)}, bf16[1088,256]{1,0:T(8,128)(2,1)}, u32[]{:S(2)}, u32[]{:S(2)}) collective-permute-start(bf16[1088,256]{1,0:T(8,128)(2,1)} %constant_dynamic-update-slice_fusion), channel_id=1, source_target_pairs={{0,4},{8,12},{16,20},{24,28},{1,5},{9,13},{17,21},{25,29},{2,6},{1... | collective-permute-start | bytes 1671176 | tf_op jit(solution)/shard_map/ppermute | solution.py:193
  14.2 3.5 %collective-permute-start.4 = (bf16[1024,256]{1,0:T(8,128)(2,1)}, bf16[1024,256]{1,0:T(8,128)(2,1)}, u32[]{:S(2)}, u32[]{:S(2)}) collective-permute-start(bf16[1024,256]{1,0:T(8,128)(2,1)} %refs_0_.3), channel_id=1, source_target_pairs={{0,8},{4,12},{8,16},{12,20},{16,24},{20,28},{1,9},{5,13},{9,17},{1... | collective-permute-start | bytes 1572872 | tf_op jit(solution)/shard_map/ppermute | solution.py:193
  25.7 5.2 %attend_own.2 = (f32[1024,128]{1,0:T(8,128)S(1)}, f32[1024,128]{1,0:T(8,128)S(1)}, f32[1024,128]{1,0:T(8,128)S(1)}) custom-call(s32[2]{0:T(128)S(1)} %get-tuple-element.30.low_ref, s32[2]{0:T(128)S(1)} %get-tuple-element.29.full_ref, s32[1]{0:T(128)} %bitcast.1.pick_ref, bf16[1024,256]{1,0:T(8,128)(2,1)S(1)} %copy-done.12, bf16[1024,256]{1,0:T(8,128)(2,1)S(1)} %copy-done.11, ...), custom_call_target="tpu_custom_call" | custom-call | flops 2147483648 | bytes 1572864 | tf_op jit(solution)/shard_map/attend_own/pallas_call | solution.py:150
  33.3 5.2 %attend_own.3 = (f32[1024,128]{1,0:T(8,128)S(1)}, f32[1024,128]{1,0:T(8,128)S(1)}, f32[1024,128]{1,0:T(8,128)S(1)}) custom-call(s32[2]{0:T(128)S(1)} %get-tuple-element.30.low_ref, s32[2]{0:T(128)S(1)} %get-tuple-element.29.full_ref, s32[1]{0:T(128)} %bitcast.1.pick_ref, bf16[1024,256]{1,0:T(8,128)(2,1)S(1)} %copy-done.12, bf16[1024,256]{1,0:T(8,128)(2,1)S(1)} %copy-done.11, ...), custom_call_target="tpu_custom_call" | custom-call | flops 2147483648 | bytes 1572864 | tf_op jit(solution)/shard_map/attend_own/pallas_call | solution.py:150
  42.6 3.5 %collective-permute-start.1 = (bf16[1088,256]{1,0:T(8,128)(2,1)}, bf16[1088,256]{1,0:T(8,128)(2,1)}, u32[]{:S(2)}, u32[]{:S(2)}) collective-permute-start(bf16[1088,256]{1,0:T(8,128)(2,1)} %collective-permute-done.refs_7_), channel_id=1, source_target_pairs={{0,4},{4,0},{8,12},{12,8},{16,20},{20,16},{24,28},{28,24},{1,5},{5... | collective-permute-start | bytes 1671176 | tf_op jit(solution)/shard_map/ppermute | solution.py:193
  50.6 9.3 %collective-permute-done.1.refs_5_.refs_9_ = bf16[1088,256]{1,0:T(8,128)(2,1)} collective-permute-done((bf16[1088,256]{1,0:T(8,128)(2,1)}, bf16[1088,256]{1,0:T(8,128)(2,1)}, u32[]{:S(2)}, u32[]{:S(2)}) %collective-permute-start.1) | collective-permute-done | bytes 557088 | tf_op jit(solution)/shard_map/ppermute | solution.py:193
  63.0 8.3 %collective-permute-start.17 = (bf16[2048,256]{1,0:T(8,128)(2,1)S(1)}, bf16[2048,256]{1,0:T(8,128)(2,1)}, u32[]{:S(2)}, u32[]{:S(2)}) collective-permute-start(bf16[2048,256]{1,0:T(8,128)(2,1)S(1)} %pad_maximum_fusion.1.refs_0_), channel_id=1, source_target_pairs={{0,8},{8,16},{16,24},{24,28},{28,20},{20,12},{12,4},{4,0},{1,9},{9... | collective-permute-start | bytes 3145736 | tf_op jit(solution)/shard_map/ppermute | solution.py:193
  73.6 7.9 %collective-permute-start.18 = (bf16[2048,256]{1,0:T(8,128)(2,1)S(1)}, bf16[2048,256]{1,0:T(8,128)(2,1)}, u32[]{:S(2)}, u32[]{:S(2)}) collective-permute-start(bf16[2048,256]{1,0:T(8,128)(2,1)S(1)} %pad_maximum_fusion.1.refs_0_), channel_id=1, source_target_pairs={{8,0},{16,8},{24,16},{28,24},{20,28},{12,20},{4,12},{0,4},{9,1},{1... | collective-permute-start | bytes 3145736 | tf_op jit(solution)/shard_map/ppermute | solution.py:193
  85.4 3.9 %collective-permute-start.6 = (bf16[1024,256]{1,0:T(8,128)(2,1)}, bf16[1024,256]{1,0:T(8,128)(2,1)S(1)}, u32[]{:S(2)}, u32[]{:S(2)}) collective-permute-start(bf16[1024,256]{1,0:T(8,128)(2,1)} %collective-permute-done.5.refs_0_.refs_4_), channel_id=1, source_target_pairs={{0,8},{8,16},{16,24},{1,9},{9,17},{17,25},{2,10},{10,18},{18,26},{... | collective-permute-start | bytes 1572872 | tf_op jit(solution)/shard_map/ppermute | solution.py:193
  89.4 15.5 %collective-permute-done.17.refs_1_ = bf16[2048,256]{1,0:T(8,128)(2,1)} collective-permute-done((bf16[2048,256]{1,0:T(8,128)(2,1)S(1)}, bf16[2048,256]{1,0:T(8,128)(2,1)}, u32[]{:S(2)}, u32[]{:S(2)}) %collective-permute-start.17) | collective-permute-done | bytes 1048608 | tf_op jit(solution)/shard_map/ppermute | solution.py:193
  104.9 4.7 %collective-permute-start.19 = (bf16[2048,256]{1,0:T(8,128)(2,1)}, bf16[2048,256]{1,0:T(8,128)(2,1)}, u32[]{:S(2)}, u32[]{:S(2)}) collective-permute-start(bf16[2048,256]{1,0:T(8,128)(2,1)} %collective-permute-done.17.refs_1_), channel_id=1, source_target_pairs={{0,8},{8,16},{16,24},{24,28},{28,20},{20,12},{12,4},{4,0},{1,9},{9... | collective-permute-start | bytes 3145736 | tf_op jit(solution)/shard_map/ppermute | solution.py:193
  109.5 6.5 %collective-permute-done.25.refs_6_ = bf16[128,2048]{1,0:T(8,128)(2,1)S(1)} collective-permute-done((bf16[128,2048]{1,0:T(8,128)(2,1)}, bf16[128,2048]{1,0:T(8,128)(2,1)S(1)}, u32[]{:S(2)}, u32[]{:S(2)}) %collective-permute-start.25) | collective-permute-done | bytes 524320 | tf_op jit(solution)/shard_map/ppermute | solution.py:193
  121.6 3.2 %attend_rest.2.refs_0_ = bf16[1024,128]{1,0:T(8,128)(2,1)S(1)} custom-call(s32[2]{0:T(128)S(1)} %get-tuple-element.47.low_ref, s32[2]{0:T(128)S(1)} %get-tuple-element.48.full_ref, s32[1]{0:T(128)} %bitcast.1.pick_ref, bf16[1024,256]{1,0:T(8,128)(2,1)S(1)} %copy-done.13, bf16[1024,256]{1,0:T(8,128)(2,1)} %collective-permute-done.5.refs_0_.refs_4_, ...), custom_call_target="tpu_custom_call" | custom-call | flops 6442450944 | bytes 1572864 | tf_op jit(solution)/shard_map/attend_rest/pallas_call | solution.py:150
  124.9 10.9 %collective-permute-start.27 = (bf16[128,2048]{1,0:T(8,128)(2,1)S(1)}, bf16[128,2048]{1,0:T(8,128)(2,1)S(1)}, u32[]{:S(2)}, u32[]{:S(2)}) collective-permute-start(bf16[128,2048]{1,0:T(8,128)(2,1)S(1)} %collective-permute-done.25.refs_6_), channel_id=1, source_target_pairs={{0,8},{8,16},{16,24},{24,28},{28,20},{20,12},{12,4},{4,0},{1,9},{9... | collective-permute-start | bytes 1572872 | tf_op jit(solution)/shard_map/ppermute | solution.py:193
  135.8 3.9 %attend_rest.3.refs_1_ = bf16[1024,128]{1,0:T(8,128)(2,1)} custom-call(s32[2]{0:T(128)S(1)} %get-tuple-element.47.low_ref, s32[2]{0:T(128)S(1)} %get-tuple-element.48.full_ref, s32[1]{0:T(128)} %bitcast.1.pick_ref, bf16[1024,256]{1,0:T(8,128)(2,1)S(1)} %copy-done.13, bf16[1024,256]{1,0:T(8,128)(2,1)} %collective-permute-done.5.refs_0_.refs_4_, ...), custom_call_target="tpu_custom_call" | custom-call | flops 6442450944 | bytes 1572864 | tf_op jit(solution)/shard_map/attend_rest/pallas_call | solution.py:150
  139.8 10.0 %collective-permute-done.27.refs_8_ = bf16[128,2048]{1,0:T(8,128)(2,1)S(1)} collective-permute-done((bf16[128,2048]{1,0:T(8,128)(2,1)S(1)}, bf16[128,2048]{1,0:T(8,128)(2,1)S(1)}, u32[]{:S(2)}, u32[]{:S(2)}) %collective-permute-start.27) | collective-permute-done | bytes 524320 | tf_op jit(solution)/shard_map/ppermute | solution.py:193
  163.0 2.5 %collective-permute-start.21 = (bf16[2048,256]{1,0:T(8,128)(2,1)}, bf16[2048,256]{1,0:T(8,128)(2,1)}, u32[]{:S(2)}, u32[]{:S(2)}) collective-permute-start(bf16[2048,256]{1,0:T(8,128)(2,1)} %collective-permute-done.19.refs_0_), channel_id=1, source_target_pairs={{0,8},{8,16},{16,24},{24,28},{28,20},{20,12},{12,4},{4,0},{1,9},{9... | collective-permute-start | bytes 3145736 | tf_op jit(solution)/shard_map/ppermute | solution.py:193
  169.8 11.5 %mix.1 = (bf16[1024,2048]{1,0:T(8,128)(2,1)}, f32[256,2048]{1,0:T(8,128)}) custom-call(s32[1]{0:T(128)} %bitcast.info_ref.block_ref, bf16[1024,128]{1,0:T(8,128)(2,1)S(1)} %attend_rest.2.refs_0_, bf16[1024,128]{1,0:T(8,128)(2,1)} %attend_rest.3.refs_1_, bf16[1024,128]{1,0:T(8,128)(2,1)S(1)} %collective-permute-done.8.refs_2_, ...), custom_call_target="tpu_custom_call" | custom-call | flops 4294967296 | bytes 16777216 | tf_op jit(solution)/shard_map/mix/pallas_call | solution.py:244
  183.6 4.5 %acts.4.refs_1_ = bf16[1024,256]{1,0:T(8,128)(2,1)S(1)} custom-call(bf16[1024,2048]{1,0:T(8,128)(2,1)S(1)} %copy-done.2, f32[1024,8]{1,0:T(8,128)S(1)} %copy.66.weight_ref, bf16[2048,256]{1,0:T(8,128)(2,1)} %collective-permute-done.19.refs_0_, bf16[2048,256]{1,0:T(8,128)(2,1)} %collective-permute-done.20.refs_1_), custom_call_target="tpu_custom_call" | custom-call | flops 2147483648 | bytes 6291456 | tf_op jit(solution)/shard_map/acts/pallas_call | solution.py:298
  188.1 5.6 %acts.3.refs_0_ = bf16[1024,384]{1,0:T(8,128)(2,1)S(1)} custom-call(bf16[1024,2048]{1,0:T(8,128)(2,1)S(1)} %copy-done.2, f32[1024,8]{1,0:T(8,128)S(1)} %copy.66.weight_ref, bf16[2048,256]{1,0:T(8,128)(2,1)S(1)} %pad_maximum_fusion.1.refs_0_, bf16[2048,256]{1,0:T(8,128)(2,1)} %collective-permute-done.17.refs_1_, bf16[2048,256]{1,0:T(8,128)(2,1)} %collective-permute-done.18.refs_2_), custom_call_target="tpu_custom_call" | custom-call | flops 3221225472 | bytes 7340032 | tf_op jit(solution)/shard_map/acts/pallas_call | solution.py:298
  198.4 4.7 %acts.5.refs_2_ = bf16[1024,256]{1,0:T(8,128)(2,1)S(1)} custom-call(bf16[1024,2048]{1,0:T(8,128)(2,1)S(1)} %copy-done.2, f32[1024,8]{1,0:T(8,128)S(1)} %copy.66.weight_ref, bf16[2048,256]{1,0:T(8,128)(2,1)} %collective-permute-done.21.refs_0_, bf16[2048,256]{1,0:T(8,128)(2,1)} %collective-permute-done.22.refs_1_), custom_call_target="tpu_custom_call" | custom-call | flops 2147483648 | bytes 6291456 | tf_op jit(solution)/shard_map/acts/pallas_call | solution.py:298
  203.1 6.8 %early.1.early_ref = bf16[1024,2048]{1,0:T(8,128)(2,1)S(1)} custom-call(bf16[1024,384]{1,0:T(8,128)(2,1)S(1)} %acts.3.refs_0_, bf16[1024,256]{1,0:T(8,128)(2,1)S(1)} %acts.4.refs_1_, bf16[1024,256]{1,0:T(8,128)(2,1)S(1)} %acts.5.refs_2_, bf16[128,2048]{1,0:T(8,128)(2,1)S(1)} %copy-done.6, bf16[128,2048]{1,0:T(8,128)(2,1)} %collective-permute-done.23.refs_4_, ...), custom_call_target="tpu_custom_call" | custom-call | flops 3758096384 | bytes 16777216 | tf_op jit(solution)/shard_map/early/pallas_call | solution.py:339
  219.2 22.5 %collective-permute-done.35 = bf16[256,2048]{1,0:T(8,128)(2,1)S(1)} collective-permute-done((bf16[256,2048]{1,0:T(8,128)(2,1)S(1)}, bf16[256,2048]{1,0:T(8,128)(2,1)S(1)}, u32[]{:S(2)}, u32[]{:S(2)}) %collective-permute-start.35) | collective-permute-done | bytes 1048608 | tf_op jit(solution)/shard_map/ppermute | solution.py:193
  (204 shorter events, 72.4 us)
Async XLA Ops:
  4.2 36.8 %collective-permute-start = (bf16[1088,256]{1,0:T(8,128)(2,1)}, bf16[1088,256]{1,0:T(8,128)(2,1)}, u32[]{:S(2)}, u32[]{:S(2)}) collective-permute-start(bf16[1088,256]{1,0:T(8,128)(2,1)} %constant_dynamic-update-slice_fusion), channel_id=1, source_target_pairs={{0,8},{4,12},{8,16},{12,20},{16,24},{20,28},{1,9},{5,13},{9,17},{1... | collective-permute-start | bytes 1671176 | tf_op jit(solution)/shard_map/ppermute | solution.py:193
  10.0 37.1 %collective-permute-start.3 = (bf16[1088,256]{1,0:T(8,128)(2,1)}, bf16[1088,256]{1,0:T(8,128)(2,1)}, u32[]{:S(2)}, u32[]{:S(2)}) collective-permute-start(bf16[1088,256]{1,0:T(8,128)(2,1)} %constant_dynamic-update-slice_fusion), channel_id=1, source_target_pairs={{0,4},{8,12},{16,20},{24,28},{1,5},{9,13},{17,21},{25,29},{2,6},{1... | collective-permute-start | bytes 1671176 | tf_op jit(solution)/shard_map/ppermute | solution.py:193
  14.2 32.8 %collective-permute-start.4 = (bf16[1024,256]{1,0:T(8,128)(2,1)}, bf16[1024,256]{1,0:T(8,128)(2,1)}, u32[]{:S(2)}, u32[]{:S(2)}) collective-permute-start(bf16[1024,256]{1,0:T(8,128)(2,1)} %refs_0_.3), channel_id=1, source_target_pairs={{0,8},{4,12},{8,16},{12,20},{16,24},{20,28},{1,9},{5,13},{9,17},{1... | collective-permute-start | bytes 1572872 | tf_op jit(solution)/shard_map/ppermute | solution.py:193
  17.7 45.3 %collective-permute-start.7 = (bf16[1024,256]{1,0:T(8,128)(2,1)}, bf16[1024,256]{1,0:T(8,128)(2,1)}, u32[]{:S(2)}, u32[]{:S(2)}) collective-permute-start(bf16[1024,256]{1,0:T(8,128)(2,1)} %refs_0_.3), channel_id=1, source_target_pairs={{0,4},{8,12},{16,20},{24,28},{1,5},{9,13},{17,21},{25,29},{2,6},{1... | collective-permute-start | bytes 1572872 | tf_op jit(solution)/shard_map/ppermute | solution.py:193
  42.6 17.3 %collective-permute-start.1 = (bf16[1088,256]{1,0:T(8,128)(2,1)}, bf16[1088,256]{1,0:T(8,128)(2,1)}, u32[]{:S(2)}, u32[]{:S(2)}) collective-permute-start(bf16[1088,256]{1,0:T(8,128)(2,1)} %collective-permute-done.refs_7_), channel_id=1, source_target_pairs={{0,4},{4,0},{8,12},{12,8},{16,20},{20,16},{24,28},{28,24},{1,5},{5... | collective-permute-start | bytes 1671176 | tf_op jit(solution)/shard_map/ppermute | solution.py:193
  47.0 36.4 %collective-permute-start.23 = (bf16[128,2048]{1,0:T(8,128)(2,1)S(1)}, bf16[128,2048]{1,0:T(8,128)(2,1)}, u32[]{:S(2)}, u32[]{:S(2)}) collective-permute-start(bf16[128,2048]{1,0:T(8,128)(2,1)S(1)} %copy-done.5), channel_id=1, source_target_pairs={{0,8},{8,16},{16,24},{24,28},{28,20},{20,12},{12,4},{4,0},{1,9},{9... | collective-permute-start | bytes 1572872 | tf_op jit(solution)/shard_map/ppermute | solution.py:193
  47.1 36.3 %collective-permute-start.24 = (bf16[128,2048]{1,0:T(8,128)(2,1)S(1)}, bf16[128,2048]{1,0:T(8,128)(2,1)}, u32[]{:S(2)}, u32[]{:S(2)}) collective-permute-start(bf16[128,2048]{1,0:T(8,128)(2,1)S(1)} %copy-done.5), channel_id=1, source_target_pairs={{8,0},{16,8},{24,16},{28,24},{20,28},{12,20},{4,12},{0,4},{9,1},{1... | collective-permute-start | bytes 1572872 | tf_op jit(solution)/shard_map/ppermute | solution.py:193
  49.1 24.4 %collective-permute-start.14 = (bf16[256,2176]{1,0:T(8,128)(2,1)S(1)}, bf16[256,2176]{1,0:T(8,128)(2,1)}, u32[]{:S(2)}, u32[]{:S(2)}) collective-permute-start(bf16[256,2176]{1,0:T(8,128)(2,1)S(1)} %pad_maximum_fusion.refs_8_), channel_id=1, source_target_pairs={{0,2},{1,3},{2,0},{3,1},{4,6},{5,7},{6,4},{7,5},{8,10},{9,11},{10,... | collective-permute-start | bytes 3342344 | tf_op jit(solution)/shard_map/ppermute | solution.py:193
  59.9 25.4 %collective-permute-start.5 = (bf16[1024,256]{1,0:T(8,128)(2,1)}, bf16[1024,256]{1,0:T(8,128)(2,1)}, u32[]{:S(2)}, u32[]{:S(2)}) collective-permute-start(bf16[1024,256]{1,0:T(8,128)(2,1)} %collective-permute-done.4.refs_2_), channel_id=1, source_target_pairs={{0,4},{4,0},{8,12},{12,8},{16,20},{20,16},{24,28},{28,24},{1,5},{5... | collective-permute-start | bytes 1572872 | tf_op jit(solution)/shard_map/ppermute | solution.py:193
  63.0 41.9 %collective-permute-start.17 = (bf16[2048,256]{1,0:T(8,128)(2,1)S(1)}, bf16[2048,256]{1,0:T(8,128)(2,1)}, u32[]{:S(2)}, u32[]{:S(2)}) collective-permute-start(bf16[2048,256]{1,0:T(8,128)(2,1)S(1)} %pad_maximum_fusion.1.refs_0_), channel_id=1, source_target_pairs={{0,8},{8,16},{16,24},{24,28},{28,20},{20,12},{12,4},{4,0},{1,9},{9... | collective-permute-start | bytes 3145736 | tf_op jit(solution)/shard_map/ppermute | solution.py:193
  73.6 31.3 %collective-permute-start.18 = (bf16[2048,256]{1,0:T(8,128)(2,1)S(1)}, bf16[2048,256]{1,0:T(8,128)(2,1)}, u32[]{:S(2)}, u32[]{:S(2)}) collective-permute-start(bf16[2048,256]{1,0:T(8,128)(2,1)S(1)} %pad_maximum_fusion.1.refs_0_), channel_id=1, source_target_pairs={{8,0},{16,8},{24,16},{28,24},{20,28},{12,20},{4,12},{0,4},{9,1},{1... | collective-permute-start | bytes 3145736 | tf_op jit(solution)/shard_map/ppermute | solution.py:193
  83.4 52.4 %collective-permute-start.15 = (bf16[256,2176]{1,0:T(8,128)(2,1)S(1)}, bf16[256,2176]{1,0:T(8,128)(2,1)S(1)}, u32[]{:S(2)}, u32[]{:S(2)}) collective-permute-start(bf16[256,2176]{1,0:T(8,128)(2,1)S(1)} %pad_maximum_fusion.refs_8_), channel_id=1, source_target_pairs={{0,1},{1,0},{2,3},{3,2},{4,5},{5,4},{6,7},{7,6},{8,9},{9,8},{10,11... | collective-permute-start | bytes 3342344 | tf_op jit(solution)/shard_map/ppermute | solution.py:193
  83.4 32.6 %collective-permute-start.25 = (bf16[128,2048]{1,0:T(8,128)(2,1)}, bf16[128,2048]{1,0:T(8,128)(2,1)S(1)}, u32[]{:S(2)}, u32[]{:S(2)}) collective-permute-start(bf16[128,2048]{1,0:T(8,128)(2,1)} %collective-permute-done.23.refs_4_), channel_id=1, source_target_pairs={{0,8},{8,16},{16,24},{24,28},{28,20},{20,12},{12,4},{4,0},{1,9},{9... | collective-permute-start | bytes 1572872 | tf_op jit(solution)/shard_map/ppermute | solution.py:193
  85.4 32.0 %collective-permute-start.6 = (bf16[1024,256]{1,0:T(8,128)(2,1)}, bf16[1024,256]{1,0:T(8,128)(2,1)S(1)}, u32[]{:S(2)}, u32[]{:S(2)}) collective-permute-start(bf16[1024,256]{1,0:T(8,128)(2,1)} %collective-permute-done.5.refs_0_.refs_4_), channel_id=1, source_target_pairs={{0,8},{8,16},{16,24},{1,9},{9,17},{17,25},{2,10},{10,18},{18,26},{... | collective-permute-start | bytes 1572872 | tf_op jit(solution)/shard_map/ppermute | solution.py:193
  104.9 20.0 %collective-permute-start.26 = (bf16[128,2048]{1,0:T(8,128)(2,1)}, bf16[128,2048]{1,0:T(8,128)(2,1)S(1)}, u32[]{:S(2)}, u32[]{:S(2)}) collective-permute-start(bf16[128,2048]{1,0:T(8,128)(2,1)} %collective-permute-done.24.refs_5_), channel_id=1, source_target_pairs={{8,0},{16,8},{24,16},{28,24},{20,28},{12,20},{4,12},{0,4},{9,1},{1... | collective-permute-start | bytes 1572872 | tf_op jit(solution)/shard_map/ppermute | solution.py:193
  104.9 58.1 %collective-permute-start.19 = (bf16[2048,256]{1,0:T(8,128)(2,1)}, bf16[2048,256]{1,0:T(8,128)(2,1)}, u32[]{:S(2)}, u32[]{:S(2)}) collective-permute-start(bf16[2048,256]{1,0:T(8,128)(2,1)} %collective-permute-done.17.refs_1_), channel_id=1, source_target_pairs={{0,8},{8,16},{16,24},{24,28},{28,20},{20,12},{12,4},{4,0},{1,9},{9... | collective-permute-start | bytes 3145736 | tf_op jit(solution)/shard_map/ppermute | solution.py:193
  116.0 49.5 %collective-permute-start.20 = (bf16[2048,256]{1,0:T(8,128)(2,1)}, bf16[2048,256]{1,0:T(8,128)(2,1)}, u32[]{:S(2)}, u32[]{:S(2)}) collective-permute-start(bf16[2048,256]{1,0:T(8,128)(2,1)} %collective-permute-done.18.refs_2_), channel_id=1, source_target_pairs={{8,0},{16,8},{24,16},{28,24},{20,28},{12,20},{4,12},{0,4},{9,1},{1... | collective-permute-start | bytes 3145736 | tf_op jit(solution)/shard_map/ppermute | solution.py:193
  117.4 33.8 %collective-permute-start.16 = (bf16[256,2176]{1,0:T(8,128)(2,1)}, bf16[256,2176]{1,0:T(8,128)(2,1)}, u32[]{:S(2)}, u32[]{:S(2)}) collective-permute-start(bf16[256,2176]{1,0:T(8,128)(2,1)} %collective-permute-done.14.refs_9_), channel_id=1, source_target_pairs={{0,1},{1,0},{2,3},{3,2},{4,5},{5,4},{6,7},{7,6},{8,9},{9,8},{10,11... | collective-permute-start | bytes 3342344 | tf_op jit(solution)/shard_map/ppermute | solution.py:193
  124.9 24.8 %collective-permute-start.27 = (bf16[128,2048]{1,0:T(8,128)(2,1)S(1)}, bf16[128,2048]{1,0:T(8,128)(2,1)S(1)}, u32[]{:S(2)}, u32[]{:S(2)}) collective-permute-start(bf16[128,2048]{1,0:T(8,128)(2,1)S(1)} %collective-permute-done.25.refs_6_), channel_id=1, source_target_pairs={{0,8},{8,16},{16,24},{24,28},{28,20},{20,12},{12,4},{4,0},{1,9},{9... | collective-permute-start | bytes 1572872 | tf_op jit(solution)/shard_map/ppermute | solution.py:193
  163.0 30.8 %collective-permute-start.21 = (bf16[2048,256]{1,0:T(8,128)(2,1)}, bf16[2048,256]{1,0:T(8,128)(2,1)}, u32[]{:S(2)}, u32[]{:S(2)}) collective-permute-start(bf16[2048,256]{1,0:T(8,128)(2,1)} %collective-permute-done.19.refs_0_), channel_id=1, source_target_pairs={{0,8},{8,16},{16,24},{24,28},{28,20},{20,12},{12,4},{4,0},{1,9},{9... | collective-permute-start | bytes 3145736 | tf_op jit(solution)/shard_map/ppermute | solution.py:193
  165.5 31.5 %collective-permute-start.22 = (bf16[2048,256]{1,0:T(8,128)(2,1)}, bf16[2048,256]{1,0:T(8,128)(2,1)}, u32[]{:S(2)}, u32[]{:S(2)}) collective-permute-start(bf16[2048,256]{1,0:T(8,128)(2,1)} %collective-permute-done.20.refs_1_), channel_id=1, source_target_pairs={{8,0},{16,8},{24,16},{28,24},{20,28},{12,20},{4,12},{0,4},{9,1},{1... | collective-permute-start | bytes 3145736 | tf_op jit(solution)/shard_map/ppermute | solution.py:193
  166.5 43.5 %collective-permute-start.31 = (bf16[64,2048]{1,0:T(8,128)(2,1)}, bf16[64,2048]{1,0:T(8,128)(2,1)S(1)}, u32[]{:S(2)}, u32[]{:S(2)}) collective-permute-start(bf16[64,2048]{1,0:T(8,128)(2,1)} %slice.192), channel_id=1, source_target_pairs={{0,8},{8,16},{16,24},{24,28},{28,20},{20,12},{12,4},{4,0},{1,9},{9... | collective-permute-start | bytes 786440 | tf_op jit(solution)/shard_map/ppermute | solution.py:193
  168.6 41.4 %collective-permute-start.32 = (bf16[64,2048]{1,0:T(8,128)(2,1)}, bf16[64,2048]{1,0:T(8,128)(2,1)S(1)}, u32[]{:S(2)}, u32[]{:S(2)}) collective-permute-start(bf16[64,2048]{1,0:T(8,128)(2,1)} %slice.193), channel_id=1, source_target_pairs={{8,0},{16,8},{24,16},{28,24},{20,28},{12,20},{4,12},{0,4},{9,1},{1... | collective-permute-start | bytes 786440 | tf_op jit(solution)/shard_map/ppermute | solution.py:193
  216.6 25.1 %collective-permute-start.35 = (bf16[256,2048]{1,0:T(8,128)(2,1)S(1)}, bf16[256,2048]{1,0:T(8,128)(2,1)S(1)}, u32[]{:S(2)}, u32[]{:S(2)}) collective-permute-start(bf16[256,2048]{1,0:T(8,128)(2,1)S(1)} %add_convert_fusion.1), channel_id=1, source_target_pairs={{0,2},{1,3},{2,0},{3,1},{4,6},{5,7},{6,4},{7,5},{8,10},{9,11},{10,... | collective-permute-start | bytes 3145736 | tf_op jit(solution)/shard_map/ppermute | solution.py:193
  (48 other events, 414.8 us)
